TPU v7x, 32 devices: a whole 2x2x4 slice. The times are simulated.
32 devices in a mesh: sp: 16 (over z, y, x), tp: 2 (over core).
Axes of the slice: x: 2, y: 2, z: 4, core: 2. Of those that a mesh axis runs over, the one named last changes fastest.
Arguments:
- tokens: bfloat16 [2048, 4096], P('sp'), may hold values from -6 to 6
- norm_gain: float32 [4096], replicated, may hold values from 0.1 to 1.9
- w_query: bfloat16 [4096, 2048], P('sp', 'tp'), may hold values from -1 to 1
- w_key: bfloat16 [4096, 512], P('sp', 'tp'), may hold values from -1 to 1
- w_value: bfloat16 [4096, 512], P('sp', 'tp'), may hold values from -0.09375 to 0.09375
- w_state_in: bfloat16 [4096, 2048], P('sp', 'tp'), may hold values from -0.09375 to 0.09375
- sink_logit: float32 [32], P('tp'), may hold values from 2 to 6
- decay_rate: float32 [128, 64], P('tp'), may hold values from 0.0002 to 4
- rotation: float32 [128, 64], P('tp'), may hold values from 1 to 60
- log_step: float32 [128], P('tp'), may hold values from -5.3 to -3
- in_re: float32 [128, 64, 16], P('tp'), may hold values from -1.5 to 1.5
- in_im: float32 [128, 64, 16], P('tp'), may hold values from -1.5 to 1.5
- out_re: float32 [128, 16, 64], P('tp'), may hold values from -0.75 to 0.75
- out_im: float32 [128, 16, 64], P('tp'), may hold values from -0.75 to 0.75
- skip_gain: float32 [2048], P('tp'), may hold values from -4 to 4
- w_attn_out: bfloat16 [2048, 4096], P('tp', 'sp'), may hold values from -0.5 to 0.5
- w_state_out: bfloat16 [2048, 4096], P('tp', 'sp'), may hold values from -0.125 to 0.125
- out_gain: float32 [4096], replicated, may hold values from 0.1 to 1.9
Outputs:
- mixed: bfloat16 [2048, 4096], P(('sp', 'tp'))
All inputs are finite; a program needn't handle non-finite values.
Results may differ from a plain program's by a relative error of at most 0.015.
The roundings to bfloat16 on the way count: a program that leaves them out, or rounds other values in their place, can miss the bound.
Values may be sent and summed in bfloat16 or wider, within the bound.
A program may use at most 128 MiB of HBM per device.

v0:
```python
import math

import jax
import jax.numpy as jnp
from jax import lax
from jax.experimental import pallas as pl
from jax.experimental.pallas import tpu as pltpu
from jax.sharding import PartitionSpec as P

HEAD = 64
WINDOW = 128
SUB = 8


epsilon = 1e-06
rotary_base = 500000.0


def passed_along(value, axis, by):
    size = lax.axis_size(axis)
    pairs = [(i, i + by) for i in range(size) if 0 <= i + by < size]
    return lax.ppermute(value, axis, pairs)


def rotate(heads_block, positions):
    head_width = heads_block.shape[-1]
    half_width = head_width // 2
    frequency = rotary_base ** (-(jnp.arange(half_width, dtype=jnp.float32) * 2.0 / head_width))
    angles = positions.astype(jnp.float32)[:, None] * frequency[None, :]
    cosine = jnp.cos(angles)[:, None, :]
    sine_part = jnp.sin(angles)[:, None, :]
    lower_half = heads_block[..., :half_width]
    upper_half = heads_block[..., half_width:]
    return jnp.concatenate(
        [
            lower_half * cosine - upper_half * sine_part,
            upper_half * cosine + lower_half * sine_part,
        ],
        axis=-1,
    )


def shape_heads(query_sum, key_sum, value_sum, positions, head_width):
    row_count = query_sum.shape[0]
    kv_heads = key_sum.shape[1] // head_width
    group_size = query_sum.shape[1] // key_sum.shape[1]
    queries = rotate(
        query_sum.reshape(row_count, kv_heads * group_size, head_width), positions
    ).astype(jnp.bfloat16)
    queries = queries.reshape(row_count, kv_heads, group_size, head_width)
    key_rows = rotate(key_sum.reshape(row_count, kv_heads, head_width), positions).astype(
        jnp.bfloat16
    )
    key_rows = key_rows.reshape(row_count, kv_heads * head_width)
    value_rows = value_sum.astype(jnp.bfloat16)
    return (queries, key_rows, value_rows)


def band_attention(queries, key_rows, value_rows, sink_logit, first_row, window):
    row_count, kv_heads, group_size, head_width = queries.shape
    blocks = row_count // window
    query_blocks = queries.reshape(blocks, window, kv_heads, group_size, head_width)
    key_blocks = jnp.concatenate(
        [
            key_rows[:row_count].reshape(blocks, window, kv_heads, head_width),
            key_rows[window:].reshape(blocks, window, kv_heads, head_width),
        ],
        axis=1,
    )
    value_blocks = jnp.concatenate(
        [
            value_rows[:row_count].reshape(blocks, window, kv_heads, head_width),
            value_rows[window:].reshape(blocks, window, kv_heads, head_width),
        ],
        axis=1,
    )
    scores = jnp.einsum(
        "bqkgd,bskd->bkgqs", query_blocks, key_blocks, preferred_element_type=jnp.float32
    ) / math.sqrt(head_width)
    block_start = jnp.arange(blocks, dtype=jnp.int32)[:, None, None] * window
    query_at = first_row + block_start + jnp.arange(window, dtype=jnp.int32)[None, :, None]
    key_at = (
        first_row - window + block_start + jnp.arange(2 * window, dtype=jnp.int32)[None, None, :]
    )
    offset_gap = query_at - key_at
    visible = (offset_gap >= 0) & (offset_gap < window) & (key_at >= 0)
    scores = jnp.where(visible[:, None, None, :, :], scores, -jnp.inf)
    sink_value = sink_logit.reshape(1, kv_heads, group_size, 1, 1)
    top_score = jnp.maximum(jnp.max(scores, axis=-1, keepdims=True), sink_value)
    exponent = jnp.exp(scores - top_score)
    totals = jnp.sum(exponent, axis=-1, keepdims=True) + jnp.exp(sink_value - top_score)
    weights = (exponent / totals).astype(jnp.bfloat16)
    attended = jnp.einsum(
        "bkgqs,bskd->bqkgd", weights, value_blocks, preferred_element_type=jnp.float32
    )
    return attended.reshape(row_count, kv_heads * group_size * head_width).astype(jnp.bfloat16)


def discretize(decay_rate, rotation, log_step, in_re, in_im):
    time_step = jnp.exp(log_step)[:, None]
    lambda_re = -decay_rate
    modulus = jnp.exp(lambda_re * time_step)
    pole_re = modulus * jnp.cos(rotation * time_step)
    pole_im = modulus * jnp.sin(rotation * time_step)
    minus_one = pole_re - 1.0
    denominator = lambda_re * lambda_re + rotation * rotation
    factor_re = ((minus_one * lambda_re + pole_im * rotation) / denominator)[..., None]
    factor_im = ((pole_im * lambda_re - minus_one * rotation) / denominator)[..., None]
    drive_re = factor_re * in_re - factor_im * in_im
    drive_im = factor_re * in_im + factor_im * in_re
    return (pole_re, pole_im, drive_re, drive_im)


def complex_power(decay_rate, rotation, log_step, exponent):
    time_step = jnp.exp(log_step)[:, None]
    modulus = jnp.exp(-decay_rate * time_step * exponent)
    angle = rotation * time_step * exponent
    return (modulus * jnp.cos(angle), modulus * jnp.sin(angle))


def token_shuffle(rows, inverse):
    steps = rows // SUB
    out_row = lax.broadcasted_iota(jnp.int32, (rows, rows), 1 if inverse else 0)
    in_row = lax.broadcasted_iota(jnp.int32, (rows, rows), 0 if inverse else 1)
    token = (out_row % SUB) * steps + out_row // SUB
    return (token == in_row).astype(jnp.bfloat16)


def scan_kernel(
    u_ref, drive_ref, pole_re_ref, pole_im_ref, jump_re_ref, jump_im_ref,
    state_ref, carry_re_ref, carry_im_ref, end_re_ref, end_im_ref,
):
    rows = u_ref.shape[0]
    width = pole_re_ref.shape[-1]
    shuffle = token_shuffle(rows, False)
    shuffled = jnp.dot(shuffle, u_ref[...], preferred_element_type=jnp.float32)
    state_ref[...] = jnp.dot(
        shuffled, drive_ref[0], precision=lax.Precision.HIGHEST,
        preferred_element_type=jnp.float32,
    )
    pole_re = jnp.broadcast_to(pole_re_ref[0], (SUB, width))
    pole_im = jnp.broadcast_to(pole_im_ref[0], (SUB, width))
    now_re = jnp.zeros((SUB, width), jnp.float32)
    now_im = jnp.zeros((SUB, width), jnp.float32)
    for step in range(rows // SUB):
        at = slice(step * SUB, (step + 1) * SUB)
        new_re = pole_re * now_re - pole_im * now_im + state_ref[at, :width]
        new_im = pole_re * now_im + pole_im * now_re + state_ref[at, width:]
        state_ref[at, :width] = new_re
        state_ref[at, width:] = new_im
        now_re, now_im = new_re, new_im
    jump_re, jump_im = (jump_re_ref[0], jump_im_ref[0])
    held_re = jnp.zeros((1, width), jnp.float32)
    held_im = jnp.zeros((1, width), jnp.float32)
    for chunk in range(SUB):
        carry_re_ref[chunk : chunk + 1, :] = held_re
        carry_im_ref[chunk : chunk + 1, :] = held_im
        next_re = jump_re * held_re - jump_im * held_im + now_re[chunk : chunk + 1]
        next_im = jump_re * held_im + jump_im * held_re + now_im[chunk : chunk + 1]
        held_re, held_im = next_re, next_im
    end_re_ref[0] = held_re
    end_im_ref[0] = held_im


def readout_kernel(
    u_ref, state_ref, carry_re_ref, carry_im_ref, prior_re_ref, prior_im_ref,
    chunk_re_ref, chunk_im_ref, pole_re_ref, pole_im_ref, read_ref, skip_ref, out_ref, full_ref,
):
    rows = u_ref.shape[0]
    width = pole_re_ref.shape[-1]
    prior_re, prior_im = (prior_re_ref[0], prior_im_ref[0])
    chunk_re, chunk_im = (chunk_re_ref[...], chunk_im_ref[...])
    add_re = carry_re_ref[...] + chunk_re * prior_re - chunk_im * prior_im
    add_im = carry_im_ref[...] + chunk_re * prior_im + chunk_im * prior_re
    pole_re = jnp.broadcast_to(pole_re_ref[0], (SUB, width))
    pole_im = jnp.broadcast_to(pole_im_ref[0], (SUB, width))
    for step in range(rows // SUB):
        at = slice(step * SUB, (step + 1) * SUB)
        turned_re = pole_re * add_re - pole_im * add_im
        turned_im = pole_re * add_im + pole_im * add_re
        full_ref[at, :width] = state_ref[at, :width] + turned_re
        full_ref[at, width:] = state_ref[at, width:] + turned_im
        add_re, add_im = turned_re, turned_im
    summed = jnp.dot(
        full_ref[...], read_ref[0], precision=lax.Precision.HIGHEST,
        preferred_element_type=jnp.float32,
    )
    shuffled = jnp.dot(
        token_shuffle(rows, False), u_ref[...], preferred_element_type=jnp.float32
    )
    mixed = jax.nn.gelu(summed + skip_ref[...] * shuffled).astype(jnp.bfloat16)
    out_ref[...] = jnp.dot(
        token_shuffle(rows, True), mixed, preferred_element_type=jnp.float32
    ).astype(jnp.bfloat16)


def block_diagonal(parts):
    blocks, per, rows, columns = parts[0].shape
    same = jnp.eye(per, dtype=bool)[None, :, None, :, None]
    spread = [
        jnp.where(same, part[:, :, :, None, :], 0.0).reshape(blocks, per * rows, per * columns)
        for part in parts
    ]
    return jnp.concatenate(spread, axis=2)


def state_tables(rows, decay_rate, rotation, log_step, in_re, in_im, out_re, out_im):
    groups, states = decay_rate.shape
    group_width = in_re.shape[-1]
    per = min(groups, max(1, 128 // group_width))
    blocks, width = (groups // per, per * states)
    pole_re, pole_im, drive_re, drive_im = discretize(decay_rate, rotation, log_step, in_re, in_im)
    steps = rows // SUB

    def by_block(value):
        return value.reshape(blocks, per, *value.shape[1:])

    def flat(value):
        return value.reshape(blocks, 1, width)

    drive = block_diagonal(
        [by_block(jnp.swapaxes(drive_re, 1, 2)), by_block(jnp.swapaxes(drive_im, 1, 2))]
    )
    read = jnp.swapaxes(block_diagonal([by_block(out_re), by_block(-out_im)]), 1, 2)
    jump = complex_power(decay_rate, rotation, log_step, float(steps))
    chunk_powers = [
        complex_power(decay_rate, rotation, log_step, float(steps * c)) for c in range(SUB)
    ]
    chunk_re = jnp.stack([p[0].reshape(groups * states) for p in chunk_powers])
    chunk_im = jnp.stack([p[1].reshape(groups * states) for p in chunk_powers])
    return dict(
        drive=drive, read=read, pole_re=flat(pole_re), pole_im=flat(pole_im),
        jump_re=flat(jump[0]), jump_im=flat(jump[1]), chunk_re=chunk_re, chunk_im=chunk_im,
        blocks=blocks, width=width, channels=per * group_width,
    )


def local_scan(inputs, tables):
    rows = inputs.shape[0]
    blocks, width, channels = (tables["blocks"], tables["width"], tables["channels"])
    row_spec = pl.BlockSpec((1, 1, width), lambda b: (b, 0, 0))
    carry_spec = pl.BlockSpec((SUB, width), lambda b: (0, b))
    return pl.pallas_call(
        scan_kernel,
        grid=(blocks,),
        in_specs=[
            pl.BlockSpec((rows, channels), lambda b: (0, b)),
            pl.BlockSpec((1, channels, 2 * width), lambda b: (b, 0, 0)),
            row_spec, row_spec, row_spec, row_spec,
        ],
        out_specs=[
            pl.BlockSpec((rows, 2 * width), lambda b: (0, b)),
            carry_spec, carry_spec, row_spec, row_spec,
        ],
        out_shape=[
            jax.ShapeDtypeStruct((rows, 2 * width * blocks), jnp.float32),
            jax.ShapeDtypeStruct((SUB, width * blocks), jnp.float32),
            jax.ShapeDtypeStruct((SUB, width * blocks), jnp.float32),
            jax.ShapeDtypeStruct((blocks, 1, width), jnp.float32),
            jax.ShapeDtypeStruct((blocks, 1, width), jnp.float32),
        ],
        cost_estimate=pl.CostEstimate(
            flops=12 * rows * channels * width * blocks, bytes_accessed=10**7, transcendentals=0
        ),
    )(
        inputs, tables["drive"], tables["pole_re"], tables["pole_im"],
        tables["jump_re"], tables["jump_im"],
    )


def read_states(inputs, scanned, prior_re, prior_im, tables, skip_gain):
    rows = inputs.shape[0]
    state, carry_re, carry_im = scanned[:3]
    blocks, width, channels = (tables["blocks"], tables["width"], tables["channels"])
    row_spec = pl.BlockSpec((1, 1, width), lambda b: (b, 0, 0))
    carry_spec = pl.BlockSpec((SUB, width), lambda b: (0, b))
    return pl.pallas_call(
        readout_kernel,
        grid=(blocks,),
        in_specs=[
            pl.BlockSpec((rows, channels), lambda b: (0, b)),
            pl.BlockSpec((rows, 2 * width), lambda b: (0, b)),
            carry_spec, carry_spec, row_spec, row_spec, carry_spec, carry_spec,
            row_spec, row_spec,
            pl.BlockSpec((1, 2 * width, channels), lambda b: (b, 0, 0)),
            pl.BlockSpec((1, channels), lambda b: (0, b)),
        ],
        out_specs=pl.BlockSpec((rows, channels), lambda b: (0, b)),
        out_shape=jax.ShapeDtypeStruct((rows, channels * blocks), jnp.bfloat16),
        scratch_shapes=[pltpu.VMEM((rows, 2 * width), jnp.float32)],
        cost_estimate=pl.CostEstimate(
            flops=12 * rows * channels * width * blocks, bytes_accessed=10**7, transcendentals=0
        ),
    )(
        inputs, state, carry_re, carry_im, prior_re, prior_im,
        tables["chunk_re"], tables["chunk_im"], tables["pole_re"], tables["pole_im"],
        tables["read"], skip_gain.reshape(1, -1),
    )


def carried_state(end_re, end_im, decay_rate, rotation, log_step, rows):
    ends = jnp.stack([end_re, end_im])
    shape = end_re.shape
    size = lax.axis_size("sp")
    reach = 1
    while reach < size:
        power_re, power_im = complex_power(decay_rate, rotation, log_step, float(rows * reach))
        power_re, power_im = (power_re.reshape(shape), power_im.reshape(shape))
        prior = passed_along(ends, "sp", reach)
        ends = ends + jnp.stack(
            [
                power_re * prior[0] - power_im * prior[1],
                power_re * prior[1] + power_im * prior[0],
            ]
        )
        reach *= 2
    before = passed_along(ends, "sp", 1)
    return (before[0], before[1])


def state_branch(inputs, decay_rate, rotation, log_step, in_re, in_im, out_re, out_im, skip_gain):
    rows = inputs.shape[0]
    tables = state_tables(rows, decay_rate, rotation, log_step, in_re, in_im, out_re, out_im)
    scanned = local_scan(inputs, tables)
    prior_re, prior_im = carried_state(
        scanned[3], scanned[4], decay_rate, rotation, log_step, rows
    )
    return read_states(inputs, scanned, prior_re, prior_im, tables, skip_gain)


def earlier_window(key_rows, value_rows):
    joined = jnp.concatenate([key_rows, value_rows], axis=1)
    prior = passed_along(joined, "sp", 1)
    return jnp.concatenate([prior, joined], axis=0)


def make_adder(normed_cols):

    def add_pieces(carried, weight_pieces, row_start):
        updated = []
        for running_total, weight_piece in zip(carried, weight_pieces):
            product = lax.dot_general(
                normed_cols,
                weight_piece,
                (((0,), (0,)), ((), ())),
                preferred_element_type=jnp.float32,
            )
            updated.append(product)
        return tuple(updated)

    return add_pieces


def body(
    tokens,
    norm_gain,
    w_query,
    w_key,
    w_value,
    w_state_in,
    sink_logit,
    decay_rate,
    rotation,
    log_step,
    in_re,
    in_im,
    out_re,
    out_im,
    skip_gain,
    w_attn_out,
    w_state_out,
    out_gain,
):
    row_count = tokens.shape[0]
    window = WINDOW
    head_width = HEAD
    wide_tokens = tokens.astype(jnp.float32)
    normed = (
        wide_tokens
        * lax.rsqrt(jnp.mean(wide_tokens * wide_tokens, axis=-1, keepdims=True) + epsilon)
        * norm_gain
    ).astype(jnp.bfloat16)
    first_row = lax.axis_index("sp") * row_count
    positions = first_row + jnp.arange(row_count, dtype=jnp.int32)
    add_pieces = make_adder(jnp.transpose(normed))

    def empty_like(weight_shard):
        return jnp.zeros((row_count, weight_shard.shape[1]), jnp.float32)

    query_sum, key_sum, value_sum, input_sum = add_pieces(
        (empty_like(w_query), empty_like(w_key), empty_like(w_value), empty_like(w_state_in)),
        (
            lax.all_gather(w_query, "sp", axis=0, tiled=True),
            lax.all_gather(w_key, "sp", axis=0, tiled=True),
            lax.all_gather(w_value, "sp", axis=0, tiled=True),
            lax.all_gather(w_state_in, "sp", axis=0, tiled=True),
        ),
        jnp.int32(0),
    )
    queries, key_rows, value_rows = shape_heads(
        query_sum, key_sum, value_sum, positions, head_width
    )
    joined_rows = earlier_window(key_rows, value_rows)
    inputs = input_sum.astype(jnp.bfloat16)
    mixed_state = state_branch(
        inputs, decay_rate, rotation, log_step, in_re, in_im, out_re, out_im, skip_gain
    )
    kv_width = key_rows.shape[1]
    kv_heads = kv_width // head_width
    all_keys = joined_rows[:, :kv_width].reshape(window + row_count, kv_heads, head_width)
    all_values = joined_rows[:, kv_width:].reshape(window + row_count, kv_heads, head_width)
    attended = band_attention(queries, all_keys, all_values, sink_logit, first_row, window)
    attn_rows, state_rows = (
        lax.all_gather(w_attn_out, "sp", axis=1, tiled=True),
        lax.all_gather(w_state_out, "sp", axis=1, tiled=True),
    )
    projected = lax.psum_scatter(
        (
            jnp.dot(attended, attn_rows, preferred_element_type=jnp.float32)
            + jnp.dot(mixed_state, state_rows, preferred_element_type=jnp.float32)
        ).astype(jnp.bfloat16),
        "tp",
        scatter_dimension=0,
        tiled=True,
    ).astype(jnp.float32)
    row_scale = lax.rsqrt(jnp.mean(projected * projected, axis=-1, keepdims=True) + epsilon)
    return (projected * row_scale * out_gain).astype(jnp.bfloat16)


def solution(mesh):
    return jax.shard_map(
        body,
        mesh=mesh,
        in_specs=(
            P("sp", None),
            P(),
            P("sp", "tp"),
            P("sp", "tp"),
            P("sp", "tp"),
            P("sp", "tp"),
            P("tp"),
            P("tp", None),
            P("tp", None),
            P("tp"),
            P("tp", None, None),
            P("tp", None, None),
            P("tp", None, None),
            P("tp", None, None),
            P("tp"),
            P("tp", "sp"),
            P("tp", "sp"),
            P(),
        ),
        out_specs=P(("sp", "tp"), None),
        check_vma=False,
    )
```

profile of v0, /device:TPU:0, one launch (start us, length us, event | category | flops | bytes accessed | tf_op | source)
XLA Modules:
  0.0 656.3 jit_solution(2599932197311673209)
XLA Ops:
  6.6 0.7 all-gather.7.cloned.1.call-update
  7.3 0.7 all-gather.9.cloned.1.call-update
  10.6 2.5 sine_multiply_fusion
  13.1 0.7 reshape.731.jump_re_ref
  13.8 0.7 stack_reshape.49
  14.5 0.7 reshape.732.jump_im_ref
  15.9 2.7 broadcast_in_dim.145
  18.6 3.5 broadcast_in_dim.146
  22.1 1.8 copy.46
  24.4 1.2 multiply_subtract_fusion
  25.6 2.7 broadcast_in_dim.142
  28.2 3.4 broadcast_in_dim.143
  31.7 1.9 copy.44
  33.6 2.7 broadcast_in_dim.148
  36.3 3.4 broadcast_in_dim.149
  39.7 1.9 copy.47
  41.6 2.7 broadcast_in_dim.138
  44.2 3.4 broadcast_in_dim.139
  47.7 1.8 copy.43
  49.5 5.5 broadcast_select_fusion.1
  55.0 2.3 pad_maximum_fusion
  57.2 5.4 copy.45.drive_ref
  62.6 1.5 reshape.729.pole_re_ref
  64.2 1.4 reshape.730.pole_im_ref
  65.6 1.4 reshape.740
  67.0 1.4 reshape.739
  68.5 1.4 reshape.738
  69.9 1.4 reshape.737
  71.4 1.4 reshape.736
  72.8 1.4 reshape.735
  74.3 1.4 reshape.734
  75.7 1.4 reshape.733
  77.1 1.4 stack_reshape.48
  78.6 1.4 stack_reshape.50
  80.0 0.7 stack_reshape.51
  81.7 1.6 stack.42.chunk_re_ref
  83.3 0.8 stack.43.chunk_im_ref
  84.9 2.6 fusion.27
  87.6 47.6 %all-gather.9.cloned.1.call-done = bf16[4096,256]{1,0:T(8,128)(2,1)} async-done(((bf16[256,256]{1,0:T(8,128)(2,1)}), bf16[4096,256]{1,0:T(8,128)(2,1)}) %all-gather.9.cloned.1.call-update) | async-done | bytes 2097168 | tf_op jit(solution)/shard_map/all_gather | solution.py:395
  135.3 2.2 convolution_convert_fusion.2
  138.2 3.4 collective-permute-start
  141.6 2.3 maximum_bitcast_fusion.read_ref
  144.4 104.7 %all-gather.15.cloned.1.call-done = bf16[4096,1024]{1,0:T(8,128)(2,1)} async-done(((bf16[256,1024]{1,0:T(8,128)(2,1)}), bf16[4096,1024]{1,0:T(8,128)(2,1)}) %all-gather.15.cloned.1.call-update) | async-done | bytes 8388624 | tf_op jit(solution)/shard_map/all_gather | solution.py:396
  249.2 5.4 convolution_convert_fusion.u_ref
  254.6 9.5 %shard_map.172 = (f32[128,8192]{1,0:T(8,128)}, f32[8,4096]{1,0:T(8,128)}, f32[8,4096]{1,0:T(8,128)}, f32[8,1,512]{2,1,0:T(1,128)}, f32[8,1,512]{2,1,0:T(1,128)}) custom-call(bf16[128,1024]{1,0:T(8,128)(2,1)} %convolution_convert_fusion.u_ref, f32[8,128,1024]{2,1,0:T(8,128)} %copy.45.drive_ref, f32[8,1,512]{2,1,0:T(1,128)} %reshape.729.pole_re_ref, ...), custom_call_target="tpu_custom_call" | custom-call | flops 805306368 | bytes 10000000 | tf_op jit(solution)/shard_map/pallas_call | solution.py:243
  264.1 0.8 pad_maximum_fusion.3
  264.9 3.2 collective-permute-start.1
  268.0 94.6 %all-gather.11.cloned.1.call-done = bf16[4096,1024]{1,0:T(8,128)(2,1)} async-done(((bf16[256,1024]{1,0:T(8,128)(2,1)}), bf16[4096,1024]{1,0:T(8,128)(2,1)}) %all-gather.11.cloned.1.call-update) | async-done | bytes 8388624 | tf_op jit(solution)/shard_map/all_gather | solution.py:393
  362.6 6.8 %fusion.24 = f32[128,1024]{0,1:T(8,128)S(1)} fusion(bf16[4096,1024]{1,0:T(8,128)(2,1)} %all-gather.11.cloned.1.call-done, bf16[128,4096]{1,0:T(8,128)(2,1)S(1)} %copy-done.1, f32[4096]{0:T(1024)S(1)} %copy-done.22, f32[128]{0:T(128)S(1)} %copy-done.25), kind=kOutput, calls=%fused_computation.121 | convolution fusion | flops 1075838976 | bytes 9978368 | tf_op jit(solution)/shard_map/dot_general | solution.py:342
  370.3 3.4 collective-permute-start.2
  374.0 1.9 collective-permute-done.2
  376.0 4.1 collective-permute-start.3
  380.2 1.6 collective-permute-done.3
  381.9 7.3 %collective-permute-start.4 = (f32[2,8,1,512]{3,2,1,0:T(1,128)S(1)}, f32[2,8,1,512]{3,2,1,0:T(1,128)S(1)}, u32[]{:S(2)}, u32[]{:S(2)}) collective-permute-start(f32[2,8,1,512]{3,2,1,0:T(1,128)S(1)} %maximum_add_fusion.2), channel_id=1, source_target_pairs={{0,16},{2,18},{4,20},{6,22},{8,24},{10,26},{12,28},{14,30},{1,17},... | collective-permute-start | bytes 98312 | tf_op jit(solution)/shard_map/ppermute | solution.py:22
  389.8 1.1 collective-permute-done.4
  391.0 2.7 collective-permute-start.5
  393.7 104.6 %all-gather.13.cloned.1.call-done = bf16[1024,4096]{1,0:T(8,128)(2,1)} async-done(((bf16[1024,256]{1,0:T(8,128)(2,1)}), bf16[1024,4096]{1,0:T(8,128)(2,1)}) %all-gather.13.cloned.1.call-update) | async-done | bytes 8388624 | tf_op jit(solution)/shard_map/all_gather | solution.py:414
  498.2 4.7 fusion.31
  503.5 10.1 %shard_map.173 = bf16[128,1024]{1,0:T(8,128)(2,1)} custom-call(bf16[128,1024]{1,0:T(8,128)(2,1)} %convolution_convert_fusion.u_ref, f32[128,8192]{1,0:T(8,128)} %get-tuple-element.10.state_ref, f32[8,4096]{1,0:T(8,128)} %get-tuple-element.11.carry_re_ref, f32[8,4096]{1,0:T(8,128)} %get-tuple-element.12.carry_im_ref, ...), custom_call_target="tpu_custom_call" | custom-call | flops 805306368 | bytes 10000000 | tf_op jit(solution)/shard_map/pallas_call | solution.py:277
  513.6 120.0 %all-gather.17.cloned.1.call-done = bf16[1024,4096]{1,0:T(8,128)(2,1)} async-done(((bf16[1024,256]{1,0:T(8,128)(2,1)}), bf16[1024,4096]{1,0:T(8,128)(2,1)}) %all-gather.17.cloned.1.call-update) | async-done | bytes 8388624 | tf_op jit(solution)/shard_map/all_gather | solution.py:415
  633.6 5.7 fusion
  639.4 6.7 %reduce-scatter.2.cloned.1.call-done = bf16[64,4096]{1,0:T(8,128)(2,1)} async-done(((bf16[128,4096]{1,0:T(8,128)(2,1)}), bf16[64,4096]{1,0:T(8,128)(2,1)}) %reduce-scatter.2.cloned.1.call-update) | async-done | bytes 524304 | tf_op jit(solution)/shard_map/reduce_scatter | solution.py:417
  646.1 1.2 fusion.5
  647.4 2.0 fusion.7
  (123 shorter events, 9.5 us)
Async XLA Ops:
  6.5 4.0 copy-start.27
  6.5 4.0 copy-start.19
  6.5 4.1 copy-start.20
  6.5 8.7 %copy-start.26 = (f32[16]{0:T(128)S(1)}, f32[16]{0:T(128)}, u32[]{:S(2)}) copy-start(f32[16]{0:T(128)} %param.24) | copy-start | bytes 196
  6.5 9.4 %copy-start.2 = (f32[64,16,64]{2,1,0:T(8,128)S(1)}, f32[64,16,64]{2,1,0:T(8,128)}, u32[]{:S(2)}) copy-start(f32[64,16,64]{2,1,0:T(8,128)} %param.30) | copy-start | bytes 786436
  6.5 78.3 %all-gather.7.cloned.1.call-start = ((), (), s32[]{:S(2)}) async-start(), calls=%async_computation.1 | async-start | bytes 2228224 | tf_op jit(solution)/shard_map/all_gather | solution.py:394
  7.3 128.0 %all-gather.9.cloned.1.call-start = ((), (), s32[]{:S(2)}) async-start(), calls=%async_computation.2 | async-start | bytes 2228224 | tf_op jit(solution)/shard_map/all_gather | solution.py:395
  8.0 241.2 %all-gather.15.cloned.1.call-start = ((), (), s32[]{:S(2)}) async-start(), calls=%async_computation.5 | async-start | bytes 8912896 | tf_op jit(solution)/shard_map/all_gather | solution.py:396
  8.8 353.9 %all-gather.11.cloned.1.call-start = ((), (), s32[]{:S(2)}) async-start(), calls=%async_computation.3 | async-start | bytes 8912896 | tf_op jit(solution)/shard_map/all_gather | solution.py:393
  9.3 488.9 %all-gather.13.cloned.1.call-start = ((), (), s32[]{:S(2)}) async-start(), calls=%async_computation.4 | async-start | bytes 8912896 | tf_op jit(solution)/shard_map/all_gather | solution.py:414
  9.9 623.7 %all-gather.17.cloned.1.call-start = ((), (), s32[]{:S(2)}) async-start(), calls=%async_computation.6 | async-start | bytes 8912896 | tf_op jit(solution)/shard_map/all_gather | solution.py:415
  10.5 635.6 %reduce-scatter.2.cloned.1.call-start = ((), (), s32[]{:S(2)}) async-start(), calls=%async_computation.7 | async-start | bytes 1572864 | tf_op jit(solution)/shard_map/reduce_scatter | solution.py:417
  22.1 2.4 copy-start.4
  31.7 1.9 copy-start.3
  57.2 22.8 %copy-start.10 = (f32[64,64]{1,0:T(8,128)S(1)}, f32[64,64]{1,0:T(8,128)}, u32[]{:S(2)}) copy-start(f32[64,64]{1,0:T(8,128)} %get-tuple-element.32) | copy-start | bytes 49156
  57.2 23.5 %copy-start.9 = (f32[64,64]{1,0:T(8,128)S(1)}, f32[64,64]{1,0:T(8,128)}, u32[]{:S(2)}) copy-start(f32[64,64]{1,0:T(8,128)} %get-tuple-element.33) | copy-start | bytes 49156
  57.2 23.6 %copy-start.8 = (f32[64,64]{1,0:T(8,128)S(1)}, f32[64,64]{1,0:T(8,128)}, u32[]{:S(2)}) copy-start(f32[64,64]{1,0:T(8,128)} %get-tuple-element.34) | copy-start | bytes 49156
  57.2 23.7 %copy-start.7 = (f32[64,64]{1,0:T(8,128)S(1)}, f32[64,64]{1,0:T(8,128)}, u32[]{:S(2)}) copy-start(f32[64,64]{1,0:T(8,128)} %get-tuple-element.35) | copy-start | bytes 49156
  62.6 21.6 %copy-start.1 = (bf16[128,4096]{1,0:T(8,128)(2,1)S(1)}, bf16[128,4096]{1,0:T(8,128)(2,1)}, u32[]{:S(2)}) copy-start(bf16[128,4096]{1,0:T(8,128)(2,1)} %param.18) | copy-start | bytes 3145732
  84.5 50.8 %copy-start.22 = (f32[4096]{0:T(1024)S(1)}, f32[4096]{0:T(1024)}, u32[]{:S(2)}) copy-start(f32[4096]{0:T(1024)} %param.19) | copy-start | bytes 49156
  84.5 53.0 %copy-start.24 = (f32[128]{0:T(128)}, f32[128]{0:T(128)S(1)}, u32[]{:S(2)}) copy-start(f32[128]{0:T(128)S(1)} %add_rsqrt_fusion.1) | copy-start | bytes 1540
  135.3 6.3 copy-start
  138.2 6.0 collective-permute-start
  254.6 108.1 %copy-start.25 = (f32[128]{0:T(128)S(1)}, f32[128]{0:T(128)}, u32[]{:S(2)}) copy-start(f32[128]{0:T(128)} %copy-done.24) | copy-start | bytes 1540
  264.9 105.3 %collective-permute-start.1 = (f32[2,8,1,512]{3,2,1,0:T(1,128)S(1)}, f32[2,8,1,512]{3,2,1,0:T(1,128)S(1)}, u32[]{:S(2)}, u32[]{:S(2)}) collective-permute-start(f32[2,8,1,512]{3,2,1,0:T(1,128)S(1)} %pad_maximum_fusion.3), channel_id=1, source_target_pairs={{0,2},{2,4},{4,6},{6,8},{8,10},{10,12},{12,14},{14,16},{16,18},{18... | collective-permute-start | bytes 98312 | tf_op jit(solution)/shard_map/ppermute | solution.py:22
  369.4 0.7 copy-start.21
  369.4 0.8 copy-start.17
  369.4 0.8 copy-start.18
  369.5 0.8 copy-start.5
  369.5 0.8 copy-start.6
  369.6 6.3 copy-start.15
  369.6 6.3 copy-start.16
  369.6 12.2 %copy-start.13 = (f32[1,8,1,512]{3,2,1,0:T(1,128)S(1)}, f32[1,8,1,512]{3,2,1,0:T(1,128)}, u32[]{:S(2)}) copy-start(f32[1,8,1,512]{3,2,1,0:T(1,128)} %reshape.738) | copy-start | bytes 49156
  369.6 12.2 %copy-start.14 = (f32[1,8,1,512]{3,2,1,0:T(1,128)S(1)}, f32[1,8,1,512]{3,2,1,0:T(1,128)}, u32[]{:S(2)}) copy-start(f32[1,8,1,512]{3,2,1,0:T(1,128)} %reshape.737) | copy-start | bytes 49156
  370.3 5.6 collective-permute-start.2
  376.0 5.8 collective-permute-start.3
  381.9 8.9 %collective-permute-start.4 = (f32[2,8,1,512]{3,2,1,0:T(1,128)S(1)}, f32[2,8,1,512]{3,2,1,0:T(1,128)S(1)}, u32[]{:S(2)}, u32[]{:S(2)}) collective-permute-start(f32[2,8,1,512]{3,2,1,0:T(1,128)S(1)} %maximum_add_fusion.2), channel_id=1, source_target_pairs={{0,16},{2,18},{4,20},{6,22},{8,24},{10,26},{12,28},{14,30},{1,17},... | collective-permute-start | bytes 98312 | tf_op jit(solution)/shard_map/ppermute | solution.py:22
  389.3 1.6 copy-start.11
  389.3 1.6 copy-start.12
  391.0 111.9 %collective-permute-start.5 = (f32[2,8,1,512]{3,2,1,0:T(1,128)S(1)}, f32[2,8,1,512]{3,2,1,0:T(1,128)S(1)}, u32[]{:S(2)}, u32[]{:S(2)}) collective-permute-start(f32[2,8,1,512]{3,2,1,0:T(1,128)S(1)} %maximum_add_fusion.3), channel_id=1, source_target_pairs={{0,2},{2,4},{4,6},{6,8},{8,10},{10,12},{12,14},{14,16},{16,18},{18... | collective-permute-start | bytes 98312 | tf_op jit(solution)/shard_map/ppermute | solution.py:22
  513.6 133.8 %copy-start.23 = (f32[4096]{0:T(1024)S(1)}, f32[4096]{0:T(1024)}, u32[]{:S(2)}) copy-start(f32[4096]{0:T(1024)} %param.35) | copy-start | bytes 49156
Sparse Core Ops, SparseCore 0:
  10.1 63.0 all-gather.6
  76.0 59.2 all-gather.8
  138.1 111.0 all-gather.14
  251.8 110.7 all-gather.10
  365.2 132.9 all-gather.12
  500.8 132.7 all-gather.16
  639.5 6.5 reduce-scatter.1
where the time goes:
time: 658 us; the launch traced here: 656 us
  waiting for transfers between devices  487 us (74%)
  local copies, waits for them, and re-layouts  63.1 us (10%)
  matrix products  28.4 us (4%)
  starting transfers between devices  24.3 us (4%)
  other arithmetic  20.1 us (3%)
  Pallas kernels  19.6 us (3%)
  between operations  14.1 us (2%)
    all_gather x1, waiting for transfers between devices, body(): lax.all_gather(w_state_out, 'sp', axis=1, tiled=True)  120 us
    all_gather x1, waiting for transfers between devices, body(): lax.all_gather(w_state_in, 'sp', axis=0, tiled=True)  105 us
    all_gather x1, waiting for transfers between devices, body(): lax.all_gather(w_attn_out, 'sp', axis=1, tiled=True)  105 us
    all_gather x1, waiting for transfers between devices, body(): lax.all_gather(w_query, 'sp', axis=0, tiled=True)  94.6 us
    all_gather x1, waiting for transfers between devices, body(): lax.all_gather(w_value, 'sp', axis=0, tiled=True)  47.6 us
    broadcast_in_dim x15, local copies, waits for them, and re-layouts, block_diagonal(): jnp.where(same, part[:, :, :, None, :], 0.0)  32.3 us
    ppermute x6, starting transfers between devices, passed_along(): return lax.ppermute(value, axis, pairs)  24 us
    dot_general x4, matrix products, add_pieces(): lax.dot_general(normed_cols, weight_piece, (((0,), (0,)), ((), ())), pref...  17 us
  transfers between devices with their start and end apart: 13, of which 10 were waited for; matrix products, arithmetic and copies ran while one was open for 16% of the time, Pallas kernels for 3%

commit v1 on v0

--- a/solution.py
+++ b/solution.py
@@ -2,6 +2,7 @@
 
 import jax
 import jax.numpy as jnp
+import numpy as np
 from jax import lax
 from jax.experimental import pallas as pl
 from jax.experimental.pallas import tpu as pltpu
@@ -351,7 +352,7 @@
     return add_pieces
 
 
-def body(
+def whole_weights_body(
     tokens,
     norm_gain,
     w_query,
@@ -427,9 +428,670 @@
     return (projected * row_scale * out_gain).astype(jnp.bfloat16)
 
 
+SIDE = 2
+PLANE = SIDE * SIDE
+CORES = 2
+LANES = 128
+MESH = pl.DeviceIdType.MESH
+
+
+def place():
+    me = lax.axis_index("sp")
+    return (lax.div(me, PLANE), lax.rem(me, PLANE), lax.axis_index("tp"))
+
+
+def plane_neighbours(spot):
+    beside = spot + 1 - 2 * lax.rem(spot, SIDE)
+    above = spot + SIDE - 2 * SIDE * lax.div(spot, SIDE)
+    return (beside, above)
+
+
+def greet(layers, layer, spot, core):
+    barrier = pltpu.get_barrier_semaphore()
+    beside, above = plane_neighbours(spot)
+    for ahead in range(1, layers):
+        other = lax.rem(layer + ahead, layers)
+        pl.semaphore_signal(
+            barrier, inc=1, device_id={"sp": other * PLANE + spot}, device_id_type=MESH
+        )
+    for other in (beside, above):
+        pl.semaphore_signal(
+            barrier, inc=1, device_id={"sp": layer * PLANE + other}, device_id_type=MESH
+        )
+    pl.semaphore_signal(barrier, inc=1, device_id={"tp": 1 - core}, device_id_type=MESH)
+    pl.semaphore_wait(barrier, layers + 2)
+
+
+def remote(source, target, send_sem, recv_sem, device):
+    return pltpu.make_async_remote_copy(
+        src_ref=source, dst_ref=target, send_sem=send_sem, recv_sem=recv_sem,
+        device_id=device, device_id_type=MESH,
+    )
+
+
+def line_first(layers, layer, spot, source, held, send_sems, recv_sems):
+    @pl.when(layer < layers - 1)
+    def _():
+        remote(
+            source, held.at[layer], send_sems.at[0, 0], recv_sems.at[0, 0],
+            {"sp": (layer + 1) * PLANE + spot},
+        ).start()
+
+    @pl.when(layer > 0)
+    def _():
+        remote(
+            source, held.at[layer], send_sems.at[1, 0], recv_sems.at[1, 0],
+            {"sp": (layer - 1) * PLANE + spot},
+        ).start()
+
+
+def line_pass(layers, layer, spot, hop, held, send_sems, recv_sems, landed=None):
+    @pl.when(layer - hop >= 0)
+    def _():
+        block = held.at[layer - hop]
+        remote(block, block, send_sems.at[0, 0], recv_sems.at[0, hop - 1], {"sp": 0}).wait_recv()
+
+        @pl.when(layer < layers - 1)
+        def _():
+            if hop < layers - 1:
+                remote(
+                    block, block, send_sems.at[0, hop], recv_sems.at[0, hop],
+                    {"sp": (layer + 1) * PLANE + spot},
+                ).start()
+
+        if landed is not None:
+            landed(0, hop, block)
+
+    @pl.when(layer + hop <= layers - 1)
+    def _():
+        block = held.at[layer + hop]
+        remote(block, block, send_sems.at[1, 0], recv_sems.at[1, hop - 1], {"sp": 0}).wait_recv()
+
+        @pl.when(layer > 0)
+        def _():
+            if hop < layers - 1:
+                remote(
+                    block, block, send_sems.at[1, hop], recv_sems.at[1, hop],
+                    {"sp": (layer - 1) * PLANE + spot},
+                ).start()
+
+        if landed is not None:
+            landed(1, hop, block)
+
+
+def line_drain(layers, layer, source, held, send_sems, recv_sems):
+    for hop in range(layers - 1):
+
+        @pl.when((layer - hop >= 0) & (layer < layers - 1))
+        def _():
+            remote(
+                source, held.at[layer], send_sems.at[0, hop], recv_sems.at[0, 0], {"sp": 0}
+            ).wait_send()
+
+        @pl.when((layer + hop <= layers - 1) & (layer > 0))
+        def _():
+            remote(
+                source, held.at[layer], send_sems.at[1, hop], recv_sems.at[1, 0], {"sp": 0}
+            ).wait_send()
+
+
+def plane_first(halves, slots, layer, spot, send_sems, recv_sems):
+    beside, above = plane_neighbours(spot)
+    copies = []
+    for half in (0, 1):
+        copies.append(
+            remote(
+                halves.at[half], slots.at[spot, half], send_sems.at[0, half],
+                recv_sems.at[0, half], {"sp": layer * PLANE + beside},
+            )
+        )
+        copies.append(
+            remote(
+                halves.at[1 - half], slots.at[spot, 1 - half], send_sems.at[1, 1 - half],
+                recv_sems.at[1, 1 - half], {"sp": layer * PLANE + above},
+            )
+        )
+    for copy in copies:
+        copy.start()
+
+
+def plane_pass(slots, layer, spot, send_sems, recv_sems):
+    beside, above = plane_neighbours(spot)
+    block = slots.at[beside, 0]
+    remote(block, block, send_sems.at[0, 0], recv_sems.at[0, 0], {"sp": 0}).wait_recv()
+    remote(
+        block, block, send_sems.at[1, 2], recv_sems.at[1, 2], {"sp": layer * PLANE + above}
+    ).start()
+    block = slots.at[above, 1]
+    remote(block, block, send_sems.at[0, 0], recv_sems.at[1, 1], {"sp": 0}).wait_recv()
+    remote(
+        block, block, send_sems.at[0, 2], recv_sems.at[0, 2], {"sp": layer * PLANE + beside}
+    ).start()
+
+
+def plane_landed(slots, spot, send_sems, recv_sems):
+    for way, half in ((0, 1), (1, 0), (0, 2), (1, 2)):
+        block = slots.at[spot, 0]
+        remote(block, block, send_sems.at[0, 0], recv_sems.at[way, half], {"sp": 0}).wait_recv()
+    for way in (0, 1):
+        for half in (0, 1, 2):
+            block = slots.at[spot, 0]
+            remote(block, block, send_sems.at[way, half], recv_sems.at[0, 0], {"sp": 0}).wait_send()
+
+
+def project_kernel(
+    packed_ref, normed_ref, row_cos_ref, row_sin_ref, block_cos_ref, block_sin_ref,
+    query_ref, pair_ref, input_ref,
+    weights, held, far_send, far_recv, line_send, line_recv, part_send, part_recv,
+    side_send, side_recv, own_sem,
+):
+    layers = packed_ref.shape[0]
+    layer, spot, core = place()
+    greet(layers, layer, spot, core)
+    for ahead in range(1, layers):
+        other = lax.rem(layer + ahead, layers)
+        remote(
+            packed_ref.at[other], weights.at[layer, spot], far_send.at[ahead], far_recv.at[ahead],
+            {"sp": other * PLANE + spot},
+        ).start()
+    plane_first(
+        packed_ref.at[layer], weights.at[layer], layer, spot, side_send.at[0], side_recv.at[0]
+    )
+    own_weights = pltpu.make_async_copy(
+        packed_ref.at[layer], weights.at[layer, spot], own_sem.at[0]
+    )
+    own_tokens = pltpu.make_async_copy(normed_ref, held.at[layer], own_sem.at[1])
+    own_weights.start()
+    own_tokens.start()
+    mine = held.at[:, core]
+    line_first(layers, layer, spot, normed_ref.at[core], mine, line_send, line_recv)
+
+    def to_partner(way, hop, block):
+        remote(
+            block, block, part_send.at[way, hop - 1], part_recv.at[way, hop - 1], {"tp": 1 - core}
+        ).start()
+
+    for ahead in range(layers):
+        origin = lax.rem(layer + layers - ahead, layers)
+        if ahead > 0:
+            block = weights.at[origin, spot]
+            remote(block, block, far_send.at[ahead], far_recv.at[ahead], {"sp": 0}).wait_recv()
+            plane_first(
+                block, weights.at[origin], layer, spot, side_send.at[ahead], side_recv.at[ahead]
+            )
+        plane_pass(weights.at[origin], layer, spot, side_send.at[ahead], side_recv.at[ahead])
+    for hop in range(1, layers):
+        line_pass(layers, layer, spot, hop, mine, line_send, line_recv, to_partner)
+    own_weights.wait()
+    own_tokens.wait()
+    for ahead in range(layers):
+        origin = lax.rem(layer + layers - ahead, layers)
+        plane_landed(weights.at[origin], spot, side_send.at[ahead], side_recv.at[ahead])
+    line_drain(layers, layer, normed_ref.at[core], mine, line_send, line_recv)
+    for hop in range(1, layers):
+        for way, there in ((0, layer - hop >= 0), (1, layer + hop <= layers - 1)):
+
+            @pl.when(there)
+            def _():
+                block = held.at[layer, 0]
+                copy = remote(
+                    block, block, part_send.at[way, hop - 1], part_recv.at[way, hop - 1],
+                    {"tp": 1 - core},
+                )
+                copy.wait_send()
+                copy.wait_recv()
+
+    for ahead in range(1, layers):
+        block = weights.at[layer, spot]
+        remote(block, block, far_send.at[ahead], far_recv.at[ahead], {"sp": 0}).wait_send()
+
+    rows = held.shape[1] * held.shape[2]
+    depth = weights.shape[2] * weights.shape[3]
+    query_width, pair_width = (query_ref.shape[-1], pair_ref.shape[-1])
+    half_width = HEAD // 2
+    lane = lax.broadcasted_iota(jnp.int32, (rows, LANES), 1)
+    low = lax.rem(lane, HEAD) < half_width
+
+    def turn(value, cosine, sine):
+        swapped = jnp.where(
+            low, -pltpu.roll(value, LANES - half_width, 1), pltpu.roll(value, half_width, 1)
+        )
+        return value * cosine + swapped * sine
+
+    @pl.loop(0, layers)
+    def _(block):
+        total = None
+        for at in range(layers * PLANE):
+            piece = jnp.dot(
+                held[block, :, :, at * depth : (at + 1) * depth].reshape(rows, depth),
+                weights[at // PLANE, at % PLANE].reshape(depth, weights.shape[-1]),
+                preferred_element_type=jnp.float32,
+            )
+            total = piece if total is None else total + piece
+        here = pl.ds(block * PLANE + spot, 1)
+        block_cos, block_sin = (block_cos_ref[here, :], block_sin_ref[here, :])
+        cosine = row_cos_ref[...] * block_cos - row_sin_ref[...] * block_sin
+        sine = row_sin_ref[...] * block_cos + row_cos_ref[...] * block_sin
+        turned = [
+            turn(total[:, at : at + LANES], cosine, sine) for at in range(0, query_width, LANES)
+        ]
+        query_ref[block] = jnp.concatenate(turned, axis=1).astype(jnp.bfloat16)
+        pairs = []
+        for at in range(query_width, query_width + pair_width, LANES):
+            value = total[:, at : at + LANES]
+            pairs.append(jnp.where(lane < HEAD, turn(value, cosine, sine), value))
+        pair_ref[block] = jnp.concatenate(pairs, axis=1).astype(jnp.bfloat16)
+        input_ref[block] = total[:, query_width + pair_width :].astype(jnp.bfloat16)
+
+
+def project(packed, normed, query_width, pair_width):
+    layers, _, half_depth, width = packed.shape
+    rows, model = normed.shape
+    half = HEAD // 2
+    frequency = rotary_base ** (-(np.arange(half) * 2.0 / HEAD))
+    frequency = np.tile(frequency, LANES // half)[None, :]
+    within = np.arange(rows)[:, None] * frequency
+    across = (np.arange(layers * PLANE) * rows)[:, None] * frequency
+    tables = [np.cos(within), np.sin(within), np.cos(across), np.sin(across)]
+    tables = [jnp.asarray(t, jnp.float32) for t in tables]
+    anywhere = pl.BlockSpec(memory_space=pl.ANY)
+    vmem = pl.BlockSpec(memory_space=pltpu.VMEM)
+    input_width = width - query_width - pair_width
+    dma = pltpu.SemaphoreType.DMA
+    return pl.pallas_call(
+        project_kernel,
+        out_shape=[
+            jax.ShapeDtypeStruct((layers, rows, query_width), jnp.bfloat16),
+            jax.ShapeDtypeStruct((layers, rows, pair_width), jnp.bfloat16),
+            jax.ShapeDtypeStruct((layers, rows, input_width), jnp.bfloat16),
+        ],
+        in_specs=[anywhere, anywhere] + [vmem] * 4,
+        out_specs=[vmem] * 3,
+        scratch_shapes=[
+            pltpu.VMEM((layers, PLANE, 2, half_depth, width), jnp.bfloat16),
+            pltpu.VMEM((layers, CORES, rows // CORES, model), jnp.bfloat16),
+            dma((layers,)), dma((layers,)),
+            dma((2, layers)), dma((2, layers)), dma((2, layers)), dma((2, layers)),
+            dma((layers, 2, 3)), dma((layers, 2, 3)), dma((2,)),
+        ],
+        compiler_params=pltpu.CompilerParams(
+            collective_id=0, has_side_effects=True, vmem_limit_bytes=48 * 2**20
+        ),
+    )(packed, normed.reshape(CORES, rows // CORES, model), *tables)
+
+
+def attend_kernel(query_ref, pair_ref, before_ref, sink_ref, out_ref):
+    block = pl.program_id(0)
+    layer, spot, core = place()
+    rows, query_width = query_ref.shape[1:]
+    group = query_width // HEAD
+    pair, before = (pair_ref[0], before_ref[0])
+    keys = jnp.concatenate([before[:, :HEAD], pair[:, :HEAD]], axis=0)
+    values = jnp.concatenate([before[:, HEAD:], pair[:, HEAD:]], axis=0)
+    query_at = lax.broadcasted_iota(jnp.int32, (rows, rows + WINDOW), 0)
+    key_at = lax.broadcasted_iota(jnp.int32, (rows, rows + WINDOW), 1) - WINDOW
+    gap = query_at - key_at
+    first = (block * PLANE + spot) * rows
+    visible = (gap >= 0) & (gap < WINDOW) & (key_at + first >= 0)
+    out = []
+    for head in range(group):
+        query = query_ref[0, :, head * HEAD : (head + 1) * HEAD]
+        scores = lax.dot_general(
+            query, keys, (((1,), (1,)), ((), ())), preferred_element_type=jnp.float32
+        ) / math.sqrt(HEAD)
+        scores = jnp.where(visible, scores, -jnp.inf)
+        sink = sink_ref[0:1, head : head + 1]
+        top = jnp.maximum(jnp.max(scores, axis=-1, keepdims=True), sink)
+        exponent = jnp.exp(scores - top)
+        total = jnp.sum(exponent, axis=-1, keepdims=True) + jnp.exp(sink - top)
+        weights = (exponent / total).astype(jnp.bfloat16)
+        out.append(jnp.dot(weights, values, preferred_element_type=jnp.float32))
+    out_ref[0] = jnp.concatenate(out, axis=1).astype(jnp.bfloat16)
+
+
+def attend(queries, pairs, before, sink):
+    layers, rows, query_width = queries.shape
+    pair_width = pairs.shape[-1]
+    flops = 4 * layers * rows * (rows + WINDOW) * query_width
+    return pl.pallas_call(
+        attend_kernel,
+        grid=(layers,),
+        in_specs=[
+            pl.BlockSpec((1, rows, query_width), lambda b: (b, 0, 0)),
+            pl.BlockSpec((1, rows, pair_width), lambda b: (b, 0, 0)),
+            pl.BlockSpec((1, rows, pair_width), lambda b: (b, 0, 0)),
+            pl.BlockSpec((1, sink.shape[-1]), lambda b: (0, 0)),
+        ],
+        out_specs=pl.BlockSpec((1, rows, query_width), lambda b: (b, 0, 0)),
+        out_shape=jax.ShapeDtypeStruct((layers, rows, query_width), jnp.bfloat16),
+        cost_estimate=pl.CostEstimate(flops=flops, bytes_accessed=10**6, transcendentals=0),
+    )(queries, pairs, before, sink)
+
+
+def output_kernel(
+    attended_ref, mixed_ref, attn_out_ref, state_out_ref, gain_ref, out_ref,
+    weights, held, partial, arrived, summed, pieces,
+    line_send, line_recv, side_send, side_recv, own_sem, half_sem, far_send, far_recv,
+):
+    layers = held.shape[0]
+    layer, spot, core = place()
+    greet(layers, layer, spot, core)
+    sources = (attended_ref, mixed_ref)
+    matrices = (attn_out_ref, state_out_ref)
+    for kind in (0, 1):
+        line_first(
+            layers, layer, spot, sources[kind], held.at[:, kind], line_send.at[kind],
+            line_recv.at[kind],
+        )
+    own = []
+    for kind in (0, 1):
+        plane_first(
+            matrices[kind], weights.at[kind], layer, spot, side_send.at[kind], side_recv.at[kind]
+        )
+        own.append(
+            pltpu.make_async_copy(matrices[kind], weights.at[kind, spot], own_sem.at[kind])
+        )
+        own.append(
+            pltpu.make_async_copy(sources[kind], held.at[layer, kind], own_sem.at[2 + kind])
+        )
+    for copy in own:
+        copy.start()
+    for hop in range(1, layers):
+        if hop < 3:
+            plane_pass(
+                weights.at[hop - 1], layer, spot, side_send.at[hop - 1], side_recv.at[hop - 1]
+            )
+        for kind in (0, 1):
+            line_pass(
+                layers, layer, spot, hop, held.at[:, kind], line_send.at[kind], line_recv.at[kind]
+            )
+    for copy in own:
+        copy.wait()
+    for kind in (0, 1):
+        plane_landed(weights.at[kind], spot, side_send.at[kind], side_recv.at[kind])
+        line_drain(
+            layers, layer, sources[kind], held.at[:, kind], line_send.at[kind], line_recv.at[kind]
+        )
+    depth = held.shape[-1]
+    tokens = held.shape[2] * held.shape[3]
+    half_depth, width = weights.shape[3:]
+    rows = partial.shape[2]
+
+    @pl.loop(0, PLANE)
+    def _(block):
+        total = None
+        for at in range(layers):
+            for kind in (0, 1):
+                low = at * depth
+                piece = jnp.dot(
+                    held[at, kind].reshape(tokens, depth),
+                    weights[kind, block, low // half_depth, pl.ds(low % half_depth, depth), :],
+                    preferred_element_type=jnp.float32,
+                )
+                total = piece if total is None else total + piece
+        rounded = total.astype(jnp.bfloat16).reshape(layers, CORES, rows, width)
+        columns = pl.ds(pl.multiple_of(block * width, width), width)
+        for half in range(CORES):
+            partial[half, :, :, columns] = rounded[:, half]
+
+    swap = remote(
+        partial.at[1 - core], arrived, half_sem.at[0], half_sem.at[1], {"tp": 1 - core}
+    )
+    swap.start()
+    swap.wait()
+    for at in range(layers):
+        summed[at] = (
+            partial[core, at].astype(jnp.float32) + arrived[at].astype(jnp.float32)
+        ).astype(jnp.bfloat16)
+    copies = []
+    for ahead in range(1, layers):
+        other = lax.rem(layer + ahead, layers)
+        copies.append(
+            remote(
+                summed.at[other], pieces.at[layer], far_send.at[ahead], far_recv.at[ahead],
+                {"sp": other * PLANE + spot},
+            )
+        )
+    for copy in copies:
+        copy.start()
+    pieces[layer] = summed[layer]
+    for copy in copies:
+        copy.wait()
+    squares = jnp.zeros((rows, 1), jnp.float32)
+    span = pieces.shape[-1]
+    for at in range(layers):
+        value = pieces[at].astype(jnp.float32)
+        squares = squares + jnp.sum(value * value, axis=-1, keepdims=True)
+    scale = lax.rsqrt(squares / (layers * span) + epsilon)
+    for at in range(layers):
+        columns = slice(at * span, (at + 1) * span)
+        out_ref[:, columns] = (
+            pieces[at].astype(jnp.float32) * scale * gain_ref[:, columns]
+        ).astype(jnp.bfloat16)
+
+
+def finish(attended, mixed, attn_out, state_out, out_gain):
+    layers, rows, depth = attended.shape
+    height, width = attn_out.shape
+    half_rows = rows // CORES
+    anywhere = pl.BlockSpec(memory_space=pl.ANY)
+    vmem = pl.BlockSpec(memory_space=pltpu.VMEM)
+    dma = pltpu.SemaphoreType.DMA
+    piece = pltpu.VMEM((layers, half_rows, PLANE * width), jnp.bfloat16)
+    return pl.pallas_call(
+        output_kernel,
+        out_shape=jax.ShapeDtypeStruct((half_rows, layers * PLANE * width), jnp.bfloat16),
+        in_specs=[anywhere] * 4 + [vmem],
+        out_specs=vmem,
+        scratch_shapes=[
+            pltpu.VMEM((2, PLANE, 2, height // 2, width), jnp.bfloat16),
+            pltpu.VMEM((layers, 2, layers, rows, depth), jnp.bfloat16),
+            pltpu.VMEM((CORES, layers, half_rows, PLANE * width), jnp.bfloat16),
+            piece, piece, piece,
+            dma((2, 2, layers)), dma((2, 2, layers)),
+            dma((2, 2, 3)), dma((2, 2, 3)), dma((4,)), dma((2,)),
+            dma((layers,)), dma((layers,)),
+        ],
+        compiler_params=pltpu.CompilerParams(
+            collective_id=1, has_side_effects=True, vmem_limit_bytes=48 * 2**20
+        ),
+    )(
+        attended, mixed, attn_out.reshape(2, height // 2, width),
+        state_out.reshape(2, height // 2, width), out_gain.reshape(1, -1),
+    )
+
+
+def blocks_scan(inputs, tables):
+    layers, rows, _ = inputs.shape
+    blocks, width, channels = (tables["blocks"], tables["width"], tables["channels"])
+    row_spec = pl.BlockSpec((1, 1, width), lambda b, t: (b, 0, 0))
+    carry_spec = pl.BlockSpec((SUB, width), lambda b, t: (t, b))
+    end_spec = pl.BlockSpec((1, 1, width), lambda b, t: (t, 0, b))
+    return pl.pallas_call(
+        scan_kernel,
+        grid=(blocks, layers),
+        in_specs=[
+            pl.BlockSpec((rows, channels), lambda b, t: (t, b)),
+            pl.BlockSpec((1, channels, 2 * width), lambda b, t: (b, 0, 0)),
+            row_spec, row_spec, row_spec, row_spec,
+        ],
+        out_specs=[
+            pl.BlockSpec((rows, 2 * width), lambda b, t: (t, b)),
+            carry_spec, carry_spec, end_spec, end_spec,
+        ],
+        out_shape=[
+            jax.ShapeDtypeStruct((layers * rows, 2 * width * blocks), jnp.float32),
+            jax.ShapeDtypeStruct((layers * SUB, width * blocks), jnp.float32),
+            jax.ShapeDtypeStruct((layers * SUB, width * blocks), jnp.float32),
+            jax.ShapeDtypeStruct((layers, 1, width * blocks), jnp.float32),
+            jax.ShapeDtypeStruct((layers, 1, width * blocks), jnp.float32),
+        ],
+        cost_estimate=pl.CostEstimate(
+            flops=12 * layers * rows * channels * width * blocks, bytes_accessed=10**7,
+            transcendentals=0,
+        ),
+    )(
+        inputs.reshape(layers * rows, -1), tables["drive"], tables["pole_re"], tables["pole_im"],
+        tables["jump_re"], tables["jump_im"],
+    )
+
+
+def blocks_read(inputs, scanned, prior_re, prior_im, tables, skip_gain):
+    layers, rows, _ = inputs.shape
+    state, carry_re, carry_im = scanned[:3]
+    blocks, width, channels = (tables["blocks"], tables["width"], tables["channels"])
+    row_spec = pl.BlockSpec((1, 1, width), lambda b, t: (b, 0, 0))
+    prior_spec = pl.BlockSpec((1, 1, width), lambda b, t: (t, 0, b))
+    carry_spec = pl.BlockSpec((SUB, width), lambda b, t: (t, b))
+    chunk_spec = pl.BlockSpec((SUB, width), lambda b, t: (0, b))
+    return pl.pallas_call(
+        readout_kernel,
+        grid=(blocks, layers),
+        in_specs=[
+            pl.BlockSpec((rows, channels), lambda b, t: (t, b)),
+            pl.BlockSpec((rows, 2 * width), lambda b, t: (t, b)),
+            carry_spec, carry_spec, prior_spec, prior_spec, chunk_spec, chunk_spec,
+            row_spec, row_spec,
+            pl.BlockSpec((1, 2 * width, channels), lambda b, t: (b, 0, 0)),
+            pl.BlockSpec((1, channels), lambda b, t: (0, b)),
+        ],
+        out_specs=pl.BlockSpec((rows, channels), lambda b, t: (t, b)),
+        out_shape=jax.ShapeDtypeStruct((layers * rows, channels * blocks), jnp.bfloat16),
+        scratch_shapes=[pltpu.VMEM((rows, 2 * width), jnp.float32)],
+        cost_estimate=pl.CostEstimate(
+            flops=12 * layers * rows * channels * width * blocks, bytes_accessed=10**7,
+            transcendentals=0,
+        ),
+    )(
+        inputs.reshape(layers * rows, -1), state, carry_re, carry_im, prior_re, prior_im,
+        tables["chunk_re"], tables["chunk_im"], tables["pole_re"], tables["pole_im"],
+        tables["read"], skip_gain.reshape(1, -1),
+    ).reshape(inputs.shape)
+
+
+def prior_states(end_re, end_im, spot, decay_rate, rotation, log_step, rows):
+    layers = end_re.shape[0]
+    size = lax.axis_size("sp")
+    planes = [[at * PLANE + other for other in range(PLANE)] for at in range(size // PLANE)]
+    ends = lax.all_gather(jnp.stack([end_re, end_im]), "sp", axis_index_groups=planes)
+    power_re, power_im = complex_power(decay_rate, rotation, log_step, float(rows))
+    power_re, power_im = (power_re.reshape(1, -1), power_im.reshape(1, -1))
+    held_re, held_im = (jnp.zeros_like(end_re[0]), jnp.zeros_like(end_im[0]))
+    prior_re, prior_im = ([], [])
+    for at in range(layers * PLANE):
+        prior_re.append(held_re)
+        prior_im.append(held_im)
+        end = ends[at % PLANE, :, at // PLANE]
+        held_re, held_im = (
+            power_re * held_re - power_im * held_im + end[0],
+            power_re * held_im + power_im * held_re + end[1],
+        )
+
+    def mine(priors):
+        stacked = jnp.stack(priors).reshape(layers, PLANE, 1, -1)
+        return lax.dynamic_index_in_dim(stacked, spot, axis=1, keepdims=False)
+
+    return (mine(prior_re), mine(prior_im))
+
+
+def body(
+    tokens,
+    norm_gain,
+    w_query,
+    w_key,
+    w_value,
+    w_state_in,
+    sink_logit,
+    decay_rate,
+    rotation,
+    log_step,
+    in_re,
+    in_im,
+    out_re,
+    out_im,
+    skip_gain,
+    w_attn_out,
+    w_state_out,
+    out_gain,
+):
+    rows = tokens.shape[0]
+    size = lax.axis_size("sp")
+    layers = size // PLANE
+    layer, spot, core = place()
+    wide_tokens = tokens.astype(jnp.float32)
+    normed = (
+        wide_tokens
+        * lax.rsqrt(jnp.mean(wide_tokens * wide_tokens, axis=-1, keepdims=True) + epsilon)
+        * norm_gain
+    ).astype(jnp.bfloat16)
+
+    def by_layer(matrix):
+        return matrix.reshape(matrix.shape[0], layers, -1)
+
+    packed = jnp.concatenate(
+        [by_layer(w_query), by_layer(w_key), by_layer(w_value), by_layer(w_state_in)], axis=2
+    )
+    depth = packed.shape[0]
+    packed = jnp.swapaxes(packed, 0, 1).reshape(layers, 2, depth // 2, -1)
+    query_width = w_query.shape[1] // layers
+    pair_width = 2 * (w_key.shape[1] // layers)
+    queries, pairs, inputs = project(packed, normed, query_width, pair_width)
+
+    passed = lax.ppermute(
+        pairs, "sp",
+        [
+            (at * PLANE + other, at * PLANE + (other + 1) % PLANE)
+            for at in range(layers)
+            for other in range(PLANE)
+        ],
+    )
+    shifted = jnp.concatenate([jnp.zeros_like(passed[:1]), passed[:-1]], axis=0)
+    before = jnp.where(spot == 0, shifted, passed)
+
+    def mine(value):
+        count = value.shape[0] // layers
+        return lax.dynamic_slice_in_dim(value, layer * count, count, 0)
+
+    decay_rate, rotation, log_step = (mine(decay_rate), mine(rotation), mine(log_step))
+    tables = state_tables(
+        rows, decay_rate, rotation, log_step, mine(in_re), mine(in_im), mine(out_re), mine(out_im)
+    )
+    scanned = blocks_scan(inputs, tables)
+    prior_re, prior_im = prior_states(
+        scanned[3], scanned[4], spot, decay_rate, rotation, log_step, rows
+    )
+    attended = attend(queries, pairs, before, mine(sink_logit).reshape(1, -1))
+    mixed = blocks_read(inputs, scanned, prior_re, prior_im, tables, mine(skip_gain))
+    return finish(attended, mixed, w_attn_out, w_state_out, out_gain)
+
+
+def suits(mesh, shapes):
+    size, cores = (mesh.shape["sp"], mesh.shape["tp"])
+    layers = size // PLANE
+    key_width = shapes[3][1] // cores
+    state_width = shapes[5][1] // cores
+    return (
+        size % PLANE == 0
+        and layers > 1
+        and cores == CORES
+        and shapes[0][0] // size == WINDOW
+        and key_width == layers * HEAD
+        and state_width % (layers * LANES) == 0
+        and shapes[2][1] % (cores * layers * LANES) == 0
+    )
+
+
 def solution(mesh):
+    def run(*arrays):
+        chosen = body if suits(mesh, [array.shape for array in arrays]) else whole_weights_body
+        return sharded(mesh, chosen)(*arrays)
+
+    return run
+
+
+def sharded(mesh, chosen):
     return jax.shard_map(
-        body,
+        chosen,
         mesh=mesh,
         in_specs=(
             P("sp", None),

time: 658 us -> 208 us (0.32)
  waiting for transfers between devices: 487 us -> 0.01 us
  Pallas kernels: 19.6 us -> 152 us
  local copies, waits for them, and re-layouts: 63.1 us -> 21.4 us
  matrix products: 28.4 us -> 0 us
  starting transfers between devices: 24.3 us -> 1.46 us
  between operations: 14.1 us -> 0.57 us
  blocking collectives: 0 us -> 9.23 us
    all_gather x6 -> x0, waiting for transfers between devices: 472 us -> none  [the longest x1 120 us: body(): lax.all_gather(w_state_out, 'sp', axis=1, tiled=True)]
    pallas_call x2 -> x5, Pallas kernels: 19.6 us -> 152 us  [the longest x1 75.3 us: project(): pl.pallas_call(project_kernel, out_shape=[jax.ShapeDtypeStruct((layers, r...]
    broadcast_in_dim x15, local copies, waits for them, and re-layouts: 32.3 us -> 2.76 us  [block_diagonal(): jnp.where(same, part[:, :, :, None, :], 0.0)]
    dot_general x8 -> x0, matrix products: 28.4 us -> none  [the longest x4 17 us: add_pieces(): lax.dot_general(normed_cols, weight_piece, (((0,), (0,)), ((), ())), pref...]
    ppermute x6 -> x1, starting transfers between devices: 24 us -> 1.46 us  [body(): lax.ppermute(pairs, 'sp', [(at * PLANE + other, at * PLANE + (other + 1)...]
    reshape x8, local copies, waits for them, and re-layouts: 11.5 us -> 1.22 us  [the longest x1 0.61 us: body(): attended = attend(queries, pairs, before, mine(sink_logit).reshape(1, -1))]
    all_gather x0 -> x1, blocking collectives: none -> 9.23 us  [prior_states(): lax.all_gather(jnp.stack([end_re, end_im]), 'sp', axis_index_groups=planes)]
    unnamed x0 -> x14, other arithmetic: none -> 8.48 us
  transfers between devices with their start and end apart: 13 -> 1, of which waited for: 10 -> 0; matrix products, arithmetic and copies ran while one was open for 16% -> 15% of each run, Pallas kernels for 3% -> 9%
where the time goes in v1:
time: 208 us; the launch traced here: 205 us
  Pallas kernels  152 us (73%)
  local copies, waits for them, and re-layouts  21.4 us (10%)
  other arithmetic  19.7 us (9%)
  blocking collectives  9.23 us (4%)
    pallas_call x1, Pallas kernels, project(): pl.pallas_call(project_kernel, out_shape=[jax.ShapeDtypeStruct((layers, r...  75.3 us
    pallas_call x1, Pallas kernels, finish(): pl.pallas_call(output_kernel, out_shape=jax.ShapeDtypeStruct((half_rows,...  51.1 us
    pallas_call x1, Pallas kernels, blocks_read(): pl.pallas_call(readout_kernel, grid=(blocks, layers), in_specs=[pl.BlockS...  9.37 us
    all_gather x1, blocking collectives, prior_states(): lax.all_gather(jnp.stack([end_re, end_im]), 'sp', axis_index_groups=planes)  9.23 us
    pallas_call x1, Pallas kernels, blocks_scan(): pl.pallas_call(scan_kernel, grid=(blocks, layers), in_specs=[pl.BlockSpec...  8.69 us
    unnamed x14, other arithmetic  8.48 us
    pallas_call x1, Pallas kernels, attend(): pl.pallas_call(attend_kernel, grid=(layers,), in_specs=[pl.BlockSpec((1,...  7.94 us
    unnamed x100, local copies, waits for them, and re-layouts  7.68 us
  transfers between devices with their start and end apart: 1, of which 0 were waited for; matrix products, arithmetic and copies ran while one was open for 15% of the time, Pallas kernels for 9%

profile of v1, /device:TPU:0, one launch (start us, length us, event | category | flops | bytes accessed | tf_op | source)
XLA Modules:
  0.0 204.8 jit_solution(5473878849200677277)
XLA Ops:
  0.0 1.1 copy.44
  1.1 0.2 copy.47
  1.3 1.1 copy.43
  2.4 0.2 copy.46
  2.6 1.5 fusion
  4.3 0.3 fusion.2
  4.7 0.3 pad_maximum_fusion
  5.1 75.3 %shard_map.208 = (bf16[4,128,256]{2,1,0:T(8,128)(2,1)S(1)}, bf16[4,128,128]{2,1,0:T(8,128)(2,1)S(1)}, bf16[4,128,256]{2,1,0:T(8,128)(2,1)S(1)}) custom-call(bf16[4,2,128,640]{3,2,1,0:T(8,128)(2,1)S(1)} %bitcast.213, bf16[2,64,4096]{2,1,0:T(8,128)(2,1)S(1)} %bitcast.214, f32[128,128]{1,0:T(8,128)S(1)} %copy-done.8, f32[128,128]{1,0:T(8,128)S(1)} %copy-done.9, ...), custom_call_target="tpu_custom_call" | custom-call | tf_op jit(solution)/shard_map/pallas_call | solution.py:701
  80.4 0.7 copy-done.5
  81.1 0.7 copy-done.6
  81.8 1.5 collective-permute-start
  83.3 0.6 constant_dynamic-update-slice_fusion.31
  84.0 0.7 sine_multiply_fusion
  84.7 0.9 sine_multiply_fusion.1
  85.6 0.7 reshape.7463.jump_re_ref
  86.3 0.7 stack_reshape.49
  87.0 0.7 reshape.7464.jump_im_ref
  87.7 1.0 dynamic-slice_negate_fusion
  88.8 0.3 broadcast_in_dim.115
  89.1 0.2 copy.54
  89.4 0.2 broadcast_in_dim.104
  89.6 0.2 copy.49
  89.8 1.0 multiply_subtract_fusion
  90.9 0.3 broadcast_in_dim.112
  91.2 0.2 copy.51
  91.5 0.3 broadcast_in_dim.118
  91.8 0.2 copy.55
  92.1 0.3 broadcast_in_dim.108
  92.4 0.2 copy.50
  92.6 0.9 broadcast_select_fusion.1
  93.6 1.3 copy.52.drive_ref
  94.9 0.7 reshape.7461.pole_re_ref
  95.6 0.7 reshape.7462.pole_im_ref
  96.4 8.7 %shard_map.210 = (f32[512,2048]{1,0:T(8,128)}, f32[32,1024]{1,0:T(8,128)}, f32[32,1024]{1,0:T(8,128)}, f32[4,1,1024]{2,1,0:T(1,128)}, f32[4,1,1024]{2,1,0:T(1,128)}) custom-call(bf16[512,256]{1,0:T(8,128)(2,1)} %bitcast.218, f32[2,128,1024]{2,1,0:T(8,128)} %copy.52.drive_ref, f32[2,1,512]{2,1,0:T(1,128)} %reshape.7461.pole_re_ref, ...), custom_call_target="tpu_custom_call" | custom-call | flops 805306368 | bytes 10000000 | tf_op jit(solution)/shard_map/pallas_call | solution.py:910
  105.1 0.8 pad_maximum_fusion.2
  105.9 9.2 %all-gather = f32[8,4,1,1024]{3,1,2,0:T(4,128)S(1)} all-gather(f32[2,4,1,1024]{3,1,2,0:T(4,128)S(1)} %copy.53), channel_id=2, replica_groups={{0,2,4,6},{8,10,12,14},{16,18,20,22},{24,26,28,30},{1,3,5,7},{9,11,13,1..., dimensions={0}, use_global_device_ids=true | all-gather | bytes 163840 | tf_op jit(solution)/shard_map/all_gather | solution.py:976
  115.4 0.4 copy-done.15
  115.8 0.8 constant_dynamic-update-slice_fusion.27
  116.5 0.8 constant_dynamic-update-slice_fusion.26
  117.3 0.8 constant_dynamic-update-slice_fusion.25
  118.1 0.8 constant_dynamic-update-slice_fusion.24
  118.8 0.8 constant_dynamic-update-slice_fusion.23
  119.6 0.8 constant_dynamic-update-slice_fusion.22
  120.4 0.8 constant_dynamic-update-slice_fusion.21
  121.1 0.8 constant_dynamic-update-slice_fusion.20
  121.9 0.8 constant_dynamic-update-slice_fusion.19
  122.7 0.8 constant_dynamic-update-slice_fusion.18
  123.4 0.8 constant_dynamic-update-slice_fusion.17
  124.2 0.8 constant_dynamic-update-slice_fusion.16
  125.1 0.7 constant_dynamic-update-slice_fusion
  126.3 0.6 dynamic-slice_bitcast_fusion.1.prior_re_ref
  126.9 0.6 dynamic-slice_bitcast_fusion.prior_im_ref
  128.6 1.1 maximum_bitcast_fusion.read_ref
  129.7 1.3 dynamic_slice.44
  131.0 0.7 stack.19.chunk_re_ref
  131.7 0.7 stack.20.chunk_im_ref
  132.3 9.4 %shard_map.211 = bf16[512,256]{1,0:T(8,128)(2,1)} custom-call(bf16[512,256]{1,0:T(8,128)(2,1)} %bitcast.219, f32[512,2048]{1,0:T(8,128)} %get-tuple-element.16.state_ref, f32[32,1024]{1,0:T(8,128)} %get-tuple-element.17.carry_re_ref, f32[32,1024]{1,0:T(8,128)} %get-tuple-element.18.carry_im_ref, f32[4,1,1024]{2,1,0:T(1,128)} %dynamic-slice_bitcast_fusion.1.prior_re_ref, ...), custom_call_target="tpu_custom_call" | custom-call | flops 805306368 | bytes 10000000 | tf_op jit(solution)/shard_map/pallas_call | solution.py:947
  141.7 0.6 dynamic-slice_bitcast_fusion.2.sink_ref
  142.3 0.7 pad_select_fusion.before_ref
  143.0 7.9 %shard_map.209.attended_ref = bf16[4,128,256]{2,1,0:T(8,128)(2,1)} custom-call(bf16[4,128,256]{2,1,0:T(8,128)(2,1)} %copy-done.6, bf16[4,128,128]{2,1,0:T(8,128)(2,1)} %copy-done.7, bf16[4,128,128]{2,1,0:T(8,128)(2,1)} %pad_select_fusion.before_ref, f32[1,4]{1,0:T(1,128)} %dynamic-slice_bitcast_fusion.2.sink_ref), custom_call_target="tpu_custom_call" | custom-call | flops 134217728 | bytes 1000000 | tf_op jit(solution)/shard_map/pallas_call | solution.py:756
  151.0 0.9 copy-done.1
  151.9 0.9 copy-done.2
  152.9 51.1 %shard_map.212 = bf16[64,4096]{1,0:T(8,128)(2,1)S(1)} custom-call(bf16[4,128,256]{2,1,0:T(8,128)(2,1)S(1)} %copy-done.2, bf16[4,128,256]{2,1,0:T(8,128)(2,1)S(1)} %bitcast.215, bf16[2,512,256]{2,1,0:T(8,128)(2,1)S(1)} %bitcast.216, bf16[2,512,256]{2,1,0:T(8,128)(2,1)S(1)} %bitcast.217, f32[1,4096]{1,0:T(1,128)S(1)} %bitcast.220), custom_call_target="tpu_custom_call" | custom-call | tf_op jit(solution)/shard_map/pallas_call | solution.py:881
  204.0 0.8 copy.93
  (128 shorter events, 3.0 us)
Async XLA Ops:
  0.0 141.7 %copy-start = (f32[16]{0:T(128)S(1)}, f32[16]{0:T(128)}, u32[]{:S(2)}) copy-start(f32[16]{0:T(128)} %param.28) | copy-start | bytes 196
  0.0 4.1 %copy-start.16 = (bf16[256,1024]{1,0:T(8,128)(2,1)S(1)}, bf16[256,1024]{1,0:T(8,128)(2,1)}, u32[]{:S(2)}) copy-start(bf16[256,1024]{1,0:T(8,128)(2,1)} %param.27) | copy-start | bytes 1572868
  0.0 4.1 %copy-start.17 = (bf16[256,1024]{1,0:T(8,128)(2,1)S(1)}, bf16[256,1024]{1,0:T(8,128)(2,1)}, u32[]{:S(2)}) copy-start(bf16[256,1024]{1,0:T(8,128)(2,1)} %param.24) | copy-start | bytes 1572868
  1.1 3.1 %copy-start.13 = (bf16[128,4096]{1,0:T(8,128)(2,1)S(1)}, bf16[128,4096]{1,0:T(8,128)(2,1)}, u32[]{:S(2)}) copy-start(bf16[128,4096]{1,0:T(8,128)(2,1)} %param.22) | copy-start | bytes 3145732
  1.1 3.1 %copy-start.36 = (f32[4096]{0:T(1024)S(1)}, f32[4096]{0:T(1024)}, u32[]{:S(2)}) copy-start(f32[4096]{0:T(1024)} %param.23) | copy-start | bytes 49156
  4.2 0.8 copy-start.8
  4.3 0.9 copy-start.9
  4.3 0.9 copy-start.11
  4.3 0.8 copy-start.12
  4.6 79.3 %copy-start.40 = (f32[64]{0:T(128)S(1)}, f32[64]{0:T(128)}, u32[]{:S(2)}) copy-start(f32[64]{0:T(128)} %param.31) | copy-start | bytes 772
  4.6 79.3 %copy-start.38 = (f32[64,64]{1,0:T(8,128)S(1)}, f32[64,64]{1,0:T(8,128)}, u32[]{:S(2)}) copy-start(f32[64,64]{1,0:T(8,128)} %param.29) | copy-start | bytes 49156
  4.6 79.3 %copy-start.39 = (f32[64,64]{1,0:T(8,128)S(1)}, f32[64,64]{1,0:T(8,128)}, u32[]{:S(2)}) copy-start(f32[64,64]{1,0:T(8,128)} %param.30) | copy-start | bytes 49156
  80.4 0.7 copy-start.5
  81.1 0.7 copy-start.6
  81.8 7.5 %copy-start.7 = (bf16[4,128,128]{2,1,0:T(8,128)(2,1)}, bf16[4,128,128]{2,1,0:T(8,128)(2,1)S(1)}, u32[]{:S(2)}) copy-start(bf16[4,128,128]{2,1,0:T(8,128)(2,1)S(1)} %get-tuple-element.14.pair_ref) | copy-start | bytes 393220
  81.8 60.5 %collective-permute-start = (bf16[4,128,128]{2,1,0:T(8,128)(2,1)S(1)}, bf16[4,128,128]{2,1,0:T(8,128)(2,1)S(1)}, u32[]{:S(2)}, u32[]{:S(2)}) collective-permute-start(bf16[4,128,128]{2,1,0:T(8,128)(2,1)S(1)} %get-tuple-element.14.pair_ref), channel_id=1, source_target_pairs={{0,2},{2,4},{4,6},{6,0},{8,10},{10,12},{12,14},{14,8},{16,18},{18,... | collective-permute-start | bytes 393224 | tf_op jit(solution)/shard_map/ppermute | solution.py:1040
  93.5 1.4 copy-start.34
  93.5 2.1 %copy-start.33 = (f32[16,64]{1,0:T(8,128)S(1)}, f32[16,64]{1,0:T(8,128)}, u32[]{:S(2)}) copy-start(f32[16,64]{1,0:T(8,128)} %get-tuple-element.92) | copy-start | bytes 12292
  94.9 20.2 %copy-start.32 = (f32[16,64]{1,0:T(8,128)S(1)}, f32[16,64]{1,0:T(8,128)}, u32[]{:S(2)}) copy-start(f32[16,64]{1,0:T(8,128)} %get-tuple-element.75) | copy-start | bytes 12292
  94.9 20.3 %copy-start.31 = (f32[16,64]{1,0:T(8,128)S(1)}, f32[16,64]{1,0:T(8,128)}, u32[]{:S(2)}) copy-start(f32[16,64]{1,0:T(8,128)} %get-tuple-element.90) | copy-start | bytes 12292
  94.9 20.3 %copy-start.18 = (f32[16,1,1024]{2,1,0:T(1,128)S(1)}, f32[16,1,1024]{2,1,0:T(1,128)}, u32[]{:S(2)}) copy-start(f32[16,1,1024]{2,1,0:T(1,128)} %constant_dynamic-update-slice_fusion.31) | copy-start | bytes 196612
  96.3 31.2 %copy-start.30 = (f32[16,64]{1,0:T(8,128)S(1)}, f32[16,64]{1,0:T(8,128)}, u32[]{:S(2)}) copy-start(f32[16,64]{1,0:T(8,128)} %get-tuple-element.89) | copy-start | bytes 12292
  96.3 31.3 %copy-start.29 = (f32[16,64]{1,0:T(8,128)S(1)}, f32[16,64]{1,0:T(8,128)}, u32[]{:S(2)}) copy-start(f32[16,64]{1,0:T(8,128)} %get-tuple-element.88) | copy-start | bytes 12292
  96.3 31.4 %copy-start.28 = (f32[16,64]{1,0:T(8,128)S(1)}, f32[16,64]{1,0:T(8,128)}, u32[]{:S(2)}) copy-start(f32[16,64]{1,0:T(8,128)} %get-tuple-element.87) | copy-start | bytes 12292
  96.3 31.4 %copy-start.27 = (f32[16,64]{1,0:T(8,128)S(1)}, f32[16,64]{1,0:T(8,128)}, u32[]{:S(2)}) copy-start(f32[16,64]{1,0:T(8,128)} %get-tuple-element.86) | copy-start | bytes 12292
  96.3 31.5 %copy-start.26 = (f32[16,64]{1,0:T(8,128)S(1)}, f32[16,64]{1,0:T(8,128)}, u32[]{:S(2)}) copy-start(f32[16,64]{1,0:T(8,128)} %get-tuple-element.85) | copy-start | bytes 12292
  96.3 31.6 %copy-start.25 = (f32[16,64]{1,0:T(8,128)S(1)}, f32[16,64]{1,0:T(8,128)}, u32[]{:S(2)}) copy-start(f32[16,64]{1,0:T(8,128)} %get-tuple-element.84) | copy-start | bytes 12292
  96.3 31.7 %copy-start.24 = (f32[16,64]{1,0:T(8,128)S(1)}, f32[16,64]{1,0:T(8,128)}, u32[]{:S(2)}) copy-start(f32[16,64]{1,0:T(8,128)} %get-tuple-element.83) | copy-start | bytes 12292
  96.3 31.7 %copy-start.23 = (f32[16,64]{1,0:T(8,128)S(1)}, f32[16,64]{1,0:T(8,128)}, u32[]{:S(2)}) copy-start(f32[16,64]{1,0:T(8,128)} %get-tuple-element.76) | copy-start | bytes 12292
  96.3 31.8 %copy-start.22 = (f32[16,64]{1,0:T(8,128)S(1)}, f32[16,64]{1,0:T(8,128)}, u32[]{:S(2)}) copy-start(f32[16,64]{1,0:T(8,128)} %get-tuple-element.77) | copy-start | bytes 12292
  96.3 31.9 %copy-start.21 = (f32[16,64]{1,0:T(8,128)S(1)}, f32[16,64]{1,0:T(8,128)}, u32[]{:S(2)}) copy-start(f32[16,64]{1,0:T(8,128)} %get-tuple-element.78) | copy-start | bytes 12292
  96.3 31.9 %copy-start.20 = (f32[16,64]{1,0:T(8,128)S(1)}, f32[16,64]{1,0:T(8,128)}, u32[]{:S(2)}) copy-start(f32[16,64]{1,0:T(8,128)} %get-tuple-element.79) | copy-start | bytes 12292
  96.4 32.0 %copy-start.19 = (f32[16,64]{1,0:T(8,128)S(1)}, f32[16,64]{1,0:T(8,128)}, u32[]{:S(2)}) copy-start(f32[16,64]{1,0:T(8,128)} %get-tuple-element.80) | copy-start | bytes 12292
  96.4 32.2 %copy-start.35 = (f32[16,64]{1,0:T(8,128)S(1)}, f32[16,64]{1,0:T(8,128)}, u32[]{:S(2)}) copy-start(f32[16,64]{1,0:T(8,128)} %get-tuple-element.21) | copy-start | bytes 12292
  96.4 32.2 %copy-start.14 = (f32[2,128,512]{1,2,0:T(8,128)S(1)}, f32[2,128,512]{1,2,0:T(8,128)}, u32[]{:S(2)}) copy-start(f32[2,128,512]{1,2,0:T(8,128)} %get-tuple-element.71) | copy-start | bytes 1572868
  105.1 25.9 %copy-start.37 = (f32[1,1024]{1,0:T(1,128)S(1)}, f32[1,1024]{1,0:T(1,128)}, u32[]{:S(2)}) copy-start(f32[1,1024]{1,0:T(1,128)} %stack_reshape.49) | copy-start | bytes 12292
  115.1 0.7 copy-start.15
  132.3 18.6 %copy-start.3 = (bf16[1024,256]{1,0:T(8,128)(2,1)S(1)}, bf16[1024,256]{1,0:T(8,128)(2,1)}, u32[]{:S(2)}) copy-start(bf16[1024,256]{1,0:T(8,128)(2,1)} %param.37) | copy-start | bytes 1572868
  132.3 18.6 %copy-start.4 = (bf16[1024,256]{1,0:T(8,128)(2,1)S(1)}, bf16[1024,256]{1,0:T(8,128)(2,1)}, u32[]{:S(2)}) copy-start(bf16[1024,256]{1,0:T(8,128)(2,1)} %param.38) | copy-start | bytes 1572868
  132.3 18.6 %copy-start.10 = (f32[4096]{0:T(1024)S(1)}, f32[4096]{0:T(1024)}, u32[]{:S(2)}) copy-start(f32[4096]{0:T(1024)} %param.39) | copy-start | bytes 49156
  151.0 1.0 copy-start.1
  151.9 0.9 copy-start.2

commit v2 on v0

--- a/solution.py
+++ b/solution.py
@@ -2,6 +2,7 @@
 
 import jax
 import jax.numpy as jnp
+import numpy as np
 from jax import lax
 from jax.experimental import pallas as pl
 from jax.experimental.pallas import tpu as pltpu
@@ -351,7 +352,7 @@
     return add_pieces
 
 
-def body(
+def whole_weights_body(
     tokens,
     norm_gain,
     w_query,
@@ -427,9 +428,854 @@
     return (projected * row_scale * out_gain).astype(jnp.bfloat16)
 
 
+SIDE = 2
+PLANE = SIDE * SIDE
+CORES = 2
+LANES = 128
+MESH = pl.DeviceIdType.MESH
+
+
+def place():
+    me = lax.axis_index("sp")
+    return (lax.div(me, PLANE), lax.rem(me, PLANE), lax.axis_index("tp"))
+
+
+def plane_neighbours(spot):
+    beside = spot + 1 - 2 * lax.rem(spot, SIDE)
+    above = spot + SIDE - 2 * SIDE * lax.div(spot, SIDE)
+    return (beside, above)
+
+
+def greet(layers, layer, spot, core):
+    barrier = pltpu.get_barrier_semaphore()
+    beside, above = plane_neighbours(spot)
+    for ahead in range(1, layers):
+        other = lax.rem(layer + ahead, layers)
+        pl.semaphore_signal(
+            barrier, inc=1, device_id={"sp": other * PLANE + spot}, device_id_type=MESH
+        )
+    for other in (beside, above, PLANE - 1 - spot):
+        pl.semaphore_signal(
+            barrier, inc=1, device_id={"sp": layer * PLANE + other}, device_id_type=MESH
+        )
+    pl.semaphore_signal(barrier, inc=1, device_id={"tp": 1 - core}, device_id_type=MESH)
+    pl.semaphore_wait(barrier, layers + 3)
+
+
+def remote(source, target, send_sem, recv_sem, device):
+    return pltpu.make_async_remote_copy(
+        src_ref=source, dst_ref=target, send_sem=send_sem, recv_sem=recv_sem,
+        device_id=device, device_id_type=MESH,
+    )
+
+
+def line_first(layers, layer, spot, source, held, send_sems, recv_sems):
+    @pl.when(layer < layers - 1)
+    def _():
+        remote(
+            source, held.at[layer], send_sems.at[0, 0], recv_sems.at[0, 0],
+            {"sp": (layer + 1) * PLANE + spot},
+        ).start()
+
+    @pl.when(layer > 0)
+    def _():
+        remote(
+            source, held.at[layer], send_sems.at[1, 0], recv_sems.at[1, 0],
+            {"sp": (layer - 1) * PLANE + spot},
+        ).start()
+
+
+def line_pass(layers, layer, spot, hop, held, send_sems, recv_sems, landed=None):
+    @pl.when(layer - hop >= 0)
+    def _():
+        block = held.at[layer - hop]
+        remote(block, block, send_sems.at[0, 0], recv_sems.at[0, hop - 1], {"sp": 0}).wait_recv()
+
+        @pl.when(layer < layers - 1)
+        def _():
+            if hop < layers - 1:
+                remote(
+                    block, block, send_sems.at[0, hop], recv_sems.at[0, hop],
+                    {"sp": (layer + 1) * PLANE + spot},
+                ).start()
+
+        if landed is not None:
+            landed(0, hop, block)
+
+    @pl.when(layer + hop <= layers - 1)
+    def _():
+        block = held.at[layer + hop]
+        remote(block, block, send_sems.at[1, 0], recv_sems.at[1, hop - 1], {"sp": 0}).wait_recv()
+
+        @pl.when(layer > 0)
+        def _():
+            if hop < layers - 1:
+                remote(
+                    block, block, send_sems.at[1, hop], recv_sems.at[1, hop],
+                    {"sp": (layer - 1) * PLANE + spot},
+                ).start()
+
+        if landed is not None:
+            landed(1, hop, block)
+
+
+def line_drain(layers, layer, source, held, send_sems, recv_sems):
+    for hop in range(layers - 1):
+
+        @pl.when((layer - hop >= 0) & (layer < layers - 1))
+        def _():
+            remote(
+                source, held.at[layer], send_sems.at[0, hop], recv_sems.at[0, 0], {"sp": 0}
+            ).wait_send()
+
+        @pl.when((layer + hop <= layers - 1) & (layer > 0))
+        def _():
+            remote(
+                source, held.at[layer], send_sems.at[1, hop], recv_sems.at[1, 0], {"sp": 0}
+            ).wait_send()
+
+
+def plane_first(halves, slots, layer, spot, send_sems, recv_sems):
+    beside, above = plane_neighbours(spot)
+    copies = []
+    for half in (0, 1):
+        copies.append(
+            remote(
+                halves.at[half], slots.at[spot, half], send_sems.at[0, half],
+                recv_sems.at[0, half], {"sp": layer * PLANE + beside},
+            )
+        )
+        copies.append(
+            remote(
+                halves.at[1 - half], slots.at[spot, 1 - half], send_sems.at[1, 1 - half],
+                recv_sems.at[1, 1 - half], {"sp": layer * PLANE + above},
+            )
+        )
+    for copy in copies:
+        copy.start()
+
+
+def plane_pass(slots, layer, spot, send_sems, recv_sems):
+    beside, above = plane_neighbours(spot)
+    block = slots.at[beside, 0]
+    remote(block, block, send_sems.at[0, 0], recv_sems.at[0, 0], {"sp": 0}).wait_recv()
+    remote(
+        block, block, send_sems.at[1, 2], recv_sems.at[1, 2], {"sp": layer * PLANE + above}
+    ).start()
+    block = slots.at[above, 1]
+    remote(block, block, send_sems.at[0, 0], recv_sems.at[1, 1], {"sp": 0}).wait_recv()
+    remote(
+        block, block, send_sems.at[0, 2], recv_sems.at[0, 2], {"sp": layer * PLANE + beside}
+    ).start()
+
+
+def plane_landed(slots, spot, send_sems, recv_sems):
+    for way, half in ((0, 1), (1, 0), (0, 2), (1, 2)):
+        block = slots.at[spot, 0]
+        remote(block, block, send_sems.at[0, 0], recv_sems.at[way, half], {"sp": 0}).wait_recv()
+    for way in (0, 1):
+        for half in (0, 1, 2):
+            block = slots.at[spot, 0]
+            remote(block, block, send_sems.at[way, half], recv_sems.at[0, 0], {"sp": 0}).wait_send()
+
+
+def lanes_of(rows):
+    return jnp.concatenate([rows[at : at + 1] for at in range(rows.shape[0])], axis=1)
+
+
+def split_pair(value):
+    high = value.astype(jnp.bfloat16)
+    return (high, (value - high.astype(jnp.float32)).astype(jnp.bfloat16))
+
+
+def make_tables(
+    layer, rows, decay_ref, rotation_ref, step_ref, in_re_ref, in_im_ref, out_re_ref, out_im_ref,
+    drive, read, powers,
+):
+    groups, states, group_width = in_re_ref.shape
+    kinds, _, width2 = drive.shape
+    per = groups // kinds
+    width = per * states
+    channels = per * group_width
+    base = layer * groups
+    decay = lanes_of(decay_ref[pl.ds(base, groups), :])
+    rotation = lanes_of(rotation_ref[pl.ds(base, groups), :])
+    step = jnp.exp(
+        jnp.concatenate(
+            [jnp.full((1, states), step_ref[base + at], jnp.float32) for at in range(groups)],
+            axis=1,
+        )
+    )
+    row = lax.broadcasted_iota(jnp.int32, (SUB, groups * states), 0)
+    steps = rows // SUB
+    shares = (row * steps, jnp.where(row == 0, 1, jnp.where(row == 1, steps, rows)))
+    for at, share in enumerate(shares):
+        share = share.astype(jnp.float32)
+        modulus = jnp.exp(-decay * step * share)
+        angle = rotation * step * share
+        powers[2 * at] = modulus * jnp.cos(angle)
+        powers[2 * at + 1] = modulus * jnp.sin(angle)
+    pole_re, pole_im = (powers[2, 0:1, :], powers[3, 0:1, :])
+    minus_one = pole_re - 1.0
+    denominator = decay * decay + rotation * rotation
+    factor_re = (pole_im * rotation - minus_one * decay) / denominator
+    factor_im = (-pole_im * decay - minus_one * rotation) / denominator
+    same = (
+        lax.broadcasted_iota(jnp.int32, (channels, width), 0) // group_width
+        == lax.broadcasted_iota(jnp.int32, (channels, width), 1) // states
+    )
+
+    def spread(pieces):
+        beside = jnp.concatenate(pieces, axis=1)
+        return jnp.concatenate([beside] * per, axis=0)
+
+    for kind in range(kinds):
+        lanes = slice(kind * width, (kind + 1) * width)
+        f_re, f_im = (factor_re[:, lanes], factor_im[:, lanes])
+        own = range(kind * per, (kind + 1) * per)
+        m_re = spread([jnp.transpose(in_re_ref[at]) for at in own])
+        m_im = spread([jnp.transpose(in_im_ref[at]) for at in own])
+        for part, value in ((0, f_re * m_re - f_im * m_im), (1, f_re * m_im + f_im * m_re)):
+            high, low = split_pair(jnp.where(same, value, 0.0))
+            columns = slice(part * width, (part + 1) * width)
+            drive[kind, :channels, columns] = high
+            drive[kind, channels:, columns] = low
+        r_re = spread([out_re_ref[at] for at in own])
+        r_im = spread([-out_im_ref[at] for at in own])
+        for part, value in ((0, r_re), (1, r_im)):
+            high, low = split_pair(jnp.where(same, value, 0.0))
+            columns = slice(part * width, (part + 1) * width)
+            read[kind, :channels, columns] = high
+            read[kind, channels:, columns] = low
+
+
+def normalise(block, held, gain_ref, normed):
+    _, parts, part_rows, model = held.shape
+    tall = 16
+    per = part_rows // tall
+
+    @pl.loop(0, parts * per)
+    def _(at):
+        value = held[
+            block, at // per, pl.ds(pl.multiple_of((at % per) * tall, tall), tall), :
+        ].astype(jnp.float32)
+        scale = lax.rsqrt(jnp.sum(value * value, axis=-1, keepdims=True) / model + epsilon)
+        normed[pl.ds(pl.multiple_of(at * tall, tall), tall), :] = (
+            value * scale * gain_ref[...]
+        ).astype(jnp.bfloat16)
+
+
+def project_block(block, spot, normed, weights, tables, queries, pairs, inputs):
+    rows, model = normed.shape
+    layers = weights.shape[0]
+    depth = weights.shape[2] * weights.shape[3]
+    query_width, pair_width = (queries.shape[-1], pairs.shape[-1])
+    half_width = HEAD // 2
+    row_cos_ref, row_sin_ref, block_cos_ref, block_sin_ref = tables
+    lane = lax.broadcasted_iota(jnp.int32, (rows, LANES), 1)
+    low = lax.rem(lane, HEAD) < half_width
+
+    def turn(value, cosine, sine):
+        swapped = jnp.where(
+            low, -pltpu.roll(value, LANES - half_width, 1), pltpu.roll(value, half_width, 1)
+        )
+        return value * cosine + swapped * sine
+
+    total = None
+    for at in range(layers * PLANE):
+        piece = jnp.dot(
+            normed[:, at * depth : (at + 1) * depth],
+            weights[at // PLANE, at % PLANE].reshape(depth, weights.shape[-1]),
+            preferred_element_type=jnp.float32,
+        )
+        total = piece if total is None else total + piece
+    here = pl.ds(block * PLANE + spot, 1)
+    block_cos, block_sin = (block_cos_ref[here, :], block_sin_ref[here, :])
+    cosine = row_cos_ref[...] * block_cos - row_sin_ref[...] * block_sin
+    sine = row_sin_ref[...] * block_cos + row_cos_ref[...] * block_sin
+    turned = [turn(total[:, at : at + LANES], cosine, sine) for at in range(0, query_width, LANES)]
+    queries[block] = jnp.concatenate(turned, axis=1).astype(jnp.bfloat16)
+    value = total[:, query_width : query_width + pair_width]
+    pairs[block] = jnp.where(lane < HEAD, turn(value, cosine, sine), value).astype(jnp.bfloat16)
+    inputs[block] = jnp.dot(
+        token_shuffle(rows, False), total[:, query_width + pair_width :].astype(jnp.bfloat16),
+        preferred_element_type=jnp.float32,
+    ).astype(jnp.bfloat16)
+
+
+def scan_block(block, spot, inputs, drive, powers, states, carries, ends):
+    kinds, _, width2 = drive.shape
+    width = width2 // 2
+    channels = inputs.shape[-1] // kinds
+    rows = inputs.shape[1]
+    for kind in range(kinds):
+        lanes = slice(kind * width, (kind + 1) * width)
+        own = inputs[block, :, kind * channels : (kind + 1) * channels]
+        states[block, kind] = jnp.dot(
+            jnp.concatenate([own, own], axis=1), drive[kind], preferred_element_type=jnp.float32
+        )
+        pole_re = jnp.broadcast_to(powers[2, 0:1, lanes], (SUB, width))
+        pole_im = jnp.broadcast_to(powers[3, 0:1, lanes], (SUB, width))
+        now_re = jnp.zeros((SUB, width), jnp.float32)
+        now_im = jnp.zeros((SUB, width), jnp.float32)
+        for step in range(rows // SUB):
+            at = slice(step * SUB, (step + 1) * SUB)
+            new_re = pole_re * now_re - pole_im * now_im + states[block, kind, at, :width]
+            new_im = pole_re * now_im + pole_im * now_re + states[block, kind, at, width:]
+            states[block, kind, at, :width] = new_re
+            states[block, kind, at, width:] = new_im
+            now_re, now_im = new_re, new_im
+        jump_re, jump_im = (powers[2, 1:2, lanes], powers[3, 1:2, lanes])
+        held_re = jnp.zeros((1, width), jnp.float32)
+        held_im = jnp.zeros((1, width), jnp.float32)
+        re, im = ([], [])
+        for chunk in range(SUB):
+            re.append(held_re)
+            im.append(held_im)
+            next_re = jump_re * held_re - jump_im * held_im + now_re[chunk : chunk + 1]
+            next_im = jump_re * held_im + jump_im * held_re + now_im[chunk : chunk + 1]
+            held_re, held_im = next_re, next_im
+        carries[block, kind, :, :width] = jnp.concatenate(re, axis=0)
+        carries[block, kind, :, width:] = jnp.concatenate(im, axis=0)
+        ends[spot, block, kind, :, :width] = held_re
+        ends[spot, block, kind, :, width:] = held_im
+
+
+def attend_block(block, layer, spot, queries, pairs, before, sink_ref, out):
+    rows, query_width = queries.shape[1:]
+    group = query_width // HEAD
+    pair, prior = (pairs[block], before[block])
+    keys = jnp.concatenate([prior[:, :HEAD], pair[:, :HEAD]], axis=0)
+    values = jnp.concatenate([prior[:, HEAD:], pair[:, HEAD:]], axis=0)
+    query_at = lax.broadcasted_iota(jnp.int32, (rows, rows + WINDOW), 0)
+    key_at = lax.broadcasted_iota(jnp.int32, (rows, rows + WINDOW), 1) - WINDOW
+    gap = query_at - key_at
+    first = (block * PLANE + spot) * rows
+    visible = (gap >= 0) & (gap < WINDOW) & (key_at + first >= 0)
+    pieces = []
+    for head in range(group):
+        query = queries[block, :, head * HEAD : (head + 1) * HEAD]
+        scores = lax.dot_general(
+            query, keys, (((1,), (1,)), ((), ())), preferred_element_type=jnp.float32
+        ) / math.sqrt(HEAD)
+        scores = jnp.where(visible, scores, -jnp.inf)
+        sink = jnp.full((1, 1), sink_ref[layer * group + head], jnp.float32)
+        top = jnp.maximum(jnp.max(scores, axis=-1, keepdims=True), sink)
+        exponent = jnp.exp(scores - top)
+        total = jnp.sum(exponent, axis=-1, keepdims=True) + jnp.exp(sink - top)
+        weights = (exponent / total).astype(jnp.bfloat16)
+        pieces.append(jnp.dot(weights, values, preferred_element_type=jnp.float32))
+    out[...] = jnp.concatenate(pieces, axis=1).astype(jnp.bfloat16)
+
+
+def find_priors(ends, powers, priors):
+    plane, layers, kinds = ends.shape[:3]
+    width = ends.shape[-1] // 2
+    for kind in range(kinds):
+        lanes = slice(kind * width, (kind + 1) * width)
+        power_re, power_im = (powers[2, 2:3, lanes], powers[3, 2:3, lanes])
+        held_re = jnp.zeros((1, width), jnp.float32)
+        held_im = jnp.zeros((1, width), jnp.float32)
+        for at in range(layers * plane):
+            priors[at, kind, :, :width] = held_re
+            priors[at, kind, :, width:] = held_im
+            end_re = ends[at % plane, at // plane, kind, :, :width]
+            end_im = ends[at % plane, at // plane, kind, :, width:]
+            held_re, held_im = (
+                power_re * held_re - power_im * held_im + end_re,
+                power_re * held_im + power_im * held_re + end_im,
+            )
+
+
+def read_block(block, layer, spot, inputs, states, carries, priors, powers, read, skip_ref, out):
+    kinds, channels2, width2 = read.shape
+    width, channels = (width2 // 2, channels2 // 2)
+    rows = inputs.shape[1]
+    contract = (((1,), (1,)), ((), ()))
+    pieces = []
+    for kind in range(kinds):
+        lanes = slice(kind * width, (kind + 1) * width)
+        prior_re = priors[block * PLANE + spot, kind, :, :width]
+        prior_im = priors[block * PLANE + spot, kind, :, width:]
+        chunk_re, chunk_im = (powers[0, :, lanes], powers[1, :, lanes])
+        add_re = carries[block, kind, :, :width] + chunk_re * prior_re - chunk_im * prior_im
+        add_im = carries[block, kind, :, width:] + chunk_re * prior_im + chunk_im * prior_re
+        pole_re = jnp.broadcast_to(powers[2, 0:1, lanes], (SUB, width))
+        pole_im = jnp.broadcast_to(powers[3, 0:1, lanes], (SUB, width))
+        for step in range(rows // SUB):
+            at = slice(step * SUB, (step + 1) * SUB)
+            turned_re = pole_re * add_re - pole_im * add_im
+            turned_im = pole_re * add_im + pole_im * add_re
+            states[block, kind, at, :width] += turned_re
+            states[block, kind, at, width:] += turned_im
+            add_re, add_im = turned_re, turned_im
+        high, low = split_pair(states[block, kind])
+        both = lax.dot_general(high, read[kind], contract, preferred_element_type=jnp.float32)
+        rest = lax.dot_general(
+            low, read[kind, :channels], contract, preferred_element_type=jnp.float32
+        )
+        summed = both[:, :channels] + both[:, channels:] + rest
+        at = pl.multiple_of(layer * (kinds * channels) + kind * channels, channels)
+        skip = skip_ref[:, pl.ds(at, channels)]
+        own = inputs[block, :, kind * channels : (kind + 1) * channels].astype(jnp.float32)
+        pieces.append(jax.nn.gelu(summed + skip * own).astype(jnp.bfloat16))
+    out[...] = jnp.dot(
+        token_shuffle(rows, True), jnp.concatenate(pieces, axis=1),
+        preferred_element_type=jnp.float32,
+    ).astype(jnp.bfloat16)
+
+
+def whole_kernel(
+    tokens_ref, query_ref, key_ref, value_ref, state_ref,
+    in_re_ref, in_im_ref, out_re_ref, out_im_ref, attn_out_ref, state_out_ref,
+    norm_gain_ref, out_gain_ref, decay_ref, rotation_ref, skip_ref,
+    row_cos_ref, row_sin_ref, block_cos_ref, block_sin_ref, step_ref, sink_ref,
+    out_ref,
+    key_value, packed, weights, held, normed, in_re, in_im, out_re, out_im, drive, read, powers,
+    queries, pairs, before, inputs, states, carries, ends, priors,
+    mixers, matrices, partial, arrived, summed, pieces,
+    load_sem, far_send, far_recv, line_send, line_recv, part_send, part_recv,
+    side_send, side_recv, halo_send, halo_recv, end_send, end_recv,
+    mixer_send, mixer_recv, matrix_send, matrix_recv, half_sem, piece_send, piece_recv,
+):
+    layers = held.shape[0]
+    rows = pairs.shape[1]
+    layer, spot, core = place()
+    query_width, pair_width = (queries.shape[-1], pairs.shape[-1])
+    state_width = inputs.shape[-1]
+    groups = in_re.shape[0]
+    mine = pl.ds(layer * groups, groups)
+    loads = [
+        pltpu.make_async_copy(key_ref, key_value.at[0], load_sem.at[0]),
+        pltpu.make_async_copy(value_ref, key_value.at[1], load_sem.at[1]),
+    ]
+    spans = (
+        (query_ref, query_width, 0, 0),
+        (state_ref, state_width, query_width + pair_width, 2),
+    )
+    own_weights = [
+        pltpu.make_async_copy(
+            source.at[:, :, pl.ds(pl.multiple_of(layer * wide, wide), wide)],
+            weights.at[layer, spot, :, :, pl.ds(to, wide)], load_sem.at[2 + at],
+        )
+        for source, wide, to, at in spans
+    ]
+    own_tokens = pltpu.make_async_copy(tokens_ref, held.at[layer], load_sem.at[3])
+    table_loads = [
+        pltpu.make_async_copy(source.at[mine], target, load_sem.at[5 + at])
+        for at, (source, target) in enumerate(
+            ((in_re_ref, in_re), (in_im_ref, in_im), (out_re_ref, out_re), (out_im_ref, out_im))
+        )
+    ]
+    matrix_loads = [
+        pltpu.make_async_copy(source, matrices.at[kind, spot], load_sem.at[9 + kind])
+        for kind, source in enumerate((attn_out_ref, state_out_ref))
+    ]
+    for copy in loads + own_weights + [own_tokens] + table_loads + matrix_loads:
+        copy.start()
+    greet(layers, layer, spot, core)
+    far = []
+    for ahead in range(1, layers):
+        other = lax.rem(layer + ahead, layers)
+        for source, wide, to, at in spans:
+            far.append(
+                remote(
+                    source.at[:, :, pl.ds(pl.multiple_of(other * wide, wide), wide)],
+                    weights.at[layer, spot, :, :, pl.ds(to, wide)],
+                    far_send.at[ahead, at], far_recv.at[ahead, at], {"sp": other * PLANE + spot},
+                )
+            )
+            far[-1].start()
+    for copy in loads:
+        copy.wait()
+    for at in range(layers):
+        head = slice(at * HEAD, (at + 1) * HEAD)
+        packed[at] = jnp.concatenate([key_value[0, :, :, head], key_value[1, :, :, head]], axis=-1)
+    middle = pl.ds(query_width, pair_width)
+    for ahead in range(1, layers):
+        other = lax.rem(layer + ahead, layers)
+        far.append(
+            remote(
+                packed.at[other], weights.at[layer, spot, :, :, middle],
+                far_send.at[ahead, 1], far_recv.at[ahead, 1], {"sp": other * PLANE + spot},
+            )
+        )
+        far[-1].start()
+    weights[layer, spot, :, :, query_width : query_width + pair_width] = packed[layer]
+    half_held = held.at[:, core]
+    line_first(layers, layer, spot, tokens_ref.at[core], half_held, line_send, line_recv)
+    for copy in own_weights:
+        copy.wait()
+    plane_first(
+        weights.at[layer, spot], weights.at[layer], layer, spot, side_send.at[0], side_recv.at[0]
+    )
+    for copy in table_loads:
+        copy.wait()
+    make_tables(
+        layer, rows, decay_ref, rotation_ref, step_ref, in_re, in_im, out_re, out_im,
+        drive, read, powers,
+    )
+    before[0] = jnp.zeros(before.shape[1:], before.dtype)
+
+    def to_partner(way, hop, block):
+        remote(
+            block, block, part_send.at[way, hop - 1], part_recv.at[way, hop - 1], {"tp": 1 - core}
+        ).start()
+
+    for ahead in range(layers):
+        origin = lax.rem(layer + layers - ahead, layers)
+        if ahead > 0:
+            for at, (to, wide) in enumerate(
+                ((0, query_width), (query_width, pair_width),
+                 (query_width + pair_width, state_width))
+            ):
+                block = weights.at[origin, spot, :, :, pl.ds(to, wide)]
+                remote(
+                    block, block, far_send.at[ahead, at], far_recv.at[ahead, at], {"sp": 0}
+                ).wait_recv()
+            plane_first(
+                weights.at[origin, spot], weights.at[origin], layer, spot,
+                side_send.at[ahead], side_recv.at[ahead],
+            )
+        plane_pass(weights.at[origin], layer, spot, side_send.at[ahead], side_recv.at[ahead])
+    for copy in matrix_loads:
+        copy.wait()
+    plane_first(
+        matrices.at[0, spot], matrices.at[0], layer, spot, matrix_send.at[0], matrix_recv.at[0]
+    )
+    line_pass(layers, layer, spot, 1, half_held, line_send, line_recv, to_partner)
+    own_tokens.wait()
+    for ahead in range(layers):
+        origin = lax.rem(layer + layers - ahead, layers)
+        plane_landed(weights.at[origin], spot, side_send.at[ahead], side_recv.at[ahead])
+    for copy in far:
+        copy.wait_send()
+
+    below, above = (layer, layers - 1 - layer)
+    least = jnp.minimum(below, above)
+    behind = layer * PLANE + lax.rem(spot + 1, PLANE)
+    late = lax.div(spot, PLANE - 1)
+
+    def hand_on(block):
+        return remote(
+            pairs.at[block], before.at[block + late], halo_send.at[block],
+            halo_recv.at[block + late], {"sp": behind},
+        )
+
+    def arrive(block):
+        remote(
+            pairs.at[0], before.at[block], halo_send.at[0], halo_recv.at[block], {"sp": behind}
+        ).wait_recv()
+
+    def tell(block, at):
+        other = lax.rem(spot + 1 + at, PLANE)
+        return remote(
+            ends.at[spot, block], ends.at[spot, block], end_send.at[at, block],
+            end_recv.at[at, block], {"sp": layer * PLANE + other},
+        )
+
+    @pl.loop(0, layers)
+    def _(at):
+        paired = at <= 2 * least
+        hop = jnp.where(paired, lax.div(at + 1, 2), at - least)
+        way = jnp.where(paired, lax.rem(at + 1, 2), jnp.where(below > above, 1, 0))
+        way = 1 - way
+        block = jnp.where(at == 0, layer, jnp.where(way == 0, layer - hop, layer + hop))
+
+        @pl.when(at > 0)
+        def _():
+            half = half_held.at[block]
+
+            @pl.when(hop > 1)
+            def _():
+                remote(
+                    half, half, line_send.at[way, 0], line_recv.at[way, hop - 1], {"sp": 0}
+                ).wait_recv()
+                onward = jnp.where(way == 0, layer < layers - 1, layer > 0)
+
+                @pl.when(onward & (hop < layers - 1))
+                def _():
+                    remote(
+                        half, half, line_send.at[way, hop], line_recv.at[way, hop],
+                        {"sp": (layer + 1 - 2 * way) * PLANE + spot},
+                    ).start()
+
+                remote(
+                    half, half, part_send.at[way, hop - 1], part_recv.at[way, hop - 1],
+                    {"tp": 1 - core},
+                ).start()
+
+            other_half = held.at[block, 1 - core]
+            remote(
+                other_half, other_half, part_send.at[way, hop - 1], part_recv.at[way, hop - 1],
+                {"tp": 1 - core},
+            ).wait_recv()
+
+        normalise(block, held, norm_gain_ref, normed)
+        project_block(
+            block, spot, normed, weights,
+            (row_cos_ref, row_sin_ref, block_cos_ref, block_sin_ref), queries, pairs, inputs,
+        )
+        hand_on(block).start()
+        scan_block(block, spot, inputs, drive, powers, states, carries, ends)
+        for peer in range(PLANE - 1):
+            tell(block, peer).start()
+
+        @pl.when((spot > 0) | (block == 0) | ((at > 0) & (way == 1)))
+        def _():
+            @pl.when((spot > 0) | (block > 0))
+            def _():
+                arrive(block)
+
+            attend_block(
+                block, layer, spot, queries, pairs, before, sink_ref, mixers.at[layer, 0, block]
+            )
+
+        @pl.when((spot == 0) & (at > 0) & (way == 0))
+        def _():
+            arrive(block + 1)
+            attend_block(
+                block + 1, layer, spot, queries, pairs, before, sink_ref,
+                mixers.at[layer, 0, block + 1],
+            )
+
+    @pl.when(spot == 0)
+    def _():
+        arrive(layers)
+
+    for kind in (0, 1):
+        if kind == 1:
+            for block in range(layers):
+                for peer in range(PLANE - 1):
+                    tell(block, peer).wait()
+            find_priors(ends, powers, priors)
+
+            @pl.loop(0, layers)
+            def _(block):
+                read_block(
+                    block, layer, spot, inputs, states, carries, priors, powers, read, skip_ref,
+                    mixers.at[layer, 1, block],
+                )
+
+        line_first(
+            layers, layer, spot, mixers.at[layer, kind], mixers.at[:, kind],
+            mixer_send.at[kind], mixer_recv.at[kind],
+        )
+    plane_pass(matrices.at[0], layer, spot, matrix_send.at[0], matrix_recv.at[0])
+    plane_first(
+        matrices.at[1, spot], matrices.at[1], layer, spot, matrix_send.at[1], matrix_recv.at[1]
+    )
+    for hop in range(1, layers):
+        for kind in (0, 1):
+            line_pass(
+                layers, layer, spot, hop, mixers.at[:, kind], mixer_send.at[kind],
+                mixer_recv.at[kind],
+            )
+        if hop == 1:
+            plane_pass(matrices.at[1], layer, spot, matrix_send.at[1], matrix_recv.at[1])
+    for kind in (0, 1):
+        plane_landed(matrices.at[kind], spot, matrix_send.at[kind], matrix_recv.at[kind])
+        line_drain(
+            layers, layer, mixers.at[layer, kind], mixers.at[:, kind], mixer_send.at[kind],
+            mixer_recv.at[kind],
+        )
+    line_drain(layers, layer, tokens_ref.at[core], half_held, line_send, line_recv)
+    for hop in range(1, layers):
+        for way, there in ((0, layer - hop >= 0), (1, layer + hop <= layers - 1)):
+
+            @pl.when(there)
+            def _():
+                block = held.at[layer, 0]
+                remote(
+                    block, block, part_send.at[way, hop - 1], part_recv.at[way, hop - 1],
+                    {"tp": 1 - core},
+                ).wait_send()
+
+    for block in range(layers):
+        hand_on(block).wait_send()
+
+    depth = mixers.shape[-1]
+    tokens = layers * rows
+    half_depth, width = matrices.shape[3:]
+    half_rows = rows // CORES
+
+    @pl.loop(0, PLANE)
+    def _(block):
+        total = None
+        for at in range(layers):
+            for kind in (0, 1):
+                low = at * depth
+                piece = jnp.dot(
+                    mixers[at, kind].reshape(tokens, depth),
+                    matrices[kind, block, low // half_depth, pl.ds(low % half_depth, depth), :],
+                    preferred_element_type=jnp.float32,
+                )
+                total = piece if total is None else total + piece
+        rounded = total.astype(jnp.bfloat16).reshape(layers, CORES, half_rows, width)
+        columns = pl.ds(pl.multiple_of(block * width, width), width)
+        for half in range(CORES):
+            partial[half, :, :, columns] = rounded[:, half]
+
+    swap = remote(
+        partial.at[1 - core], arrived, half_sem.at[0], half_sem.at[1], {"tp": 1 - core}
+    )
+    swap.start()
+    swap.wait()
+    for at in range(layers):
+        summed[at] = (
+            partial[core, at].astype(jnp.float32) + arrived[at].astype(jnp.float32)
+        ).astype(jnp.bfloat16)
+    copies = []
+    for ahead in range(1, layers):
+        other = lax.rem(layer + ahead, layers)
+        copies.append(
+            remote(
+                summed.at[other], pieces.at[layer], piece_send.at[ahead], piece_recv.at[ahead],
+                {"sp": other * PLANE + spot},
+            )
+        )
+    for copy in copies:
+        copy.start()
+    pieces[layer] = summed[layer]
+    for copy in copies:
+        copy.wait()
+    squares = jnp.zeros((half_rows, 1), jnp.float32)
+    span = pieces.shape[-1]
+    for at in range(layers):
+        value = pieces[at].astype(jnp.float32)
+        squares = squares + jnp.sum(value * value, axis=-1, keepdims=True)
+    scale = lax.rsqrt(squares / (layers * span) + epsilon)
+    for at in range(layers):
+        columns = slice(at * span, (at + 1) * span)
+        out_ref[:, columns] = (
+            pieces[at].astype(jnp.float32) * scale * out_gain_ref[:, columns]
+        ).astype(jnp.bfloat16)
+
+
+def body(
+    tokens,
+    norm_gain,
+    w_query,
+    w_key,
+    w_value,
+    w_state_in,
+    sink_logit,
+    decay_rate,
+    rotation,
+    log_step,
+    in_re,
+    in_im,
+    out_re,
+    out_im,
+    skip_gain,
+    w_attn_out,
+    w_state_out,
+    out_gain,
+):
+    rows, model = tokens.shape
+    layers = lax.axis_size("sp") // PLANE
+    half_rows = rows // CORES
+    depth = w_query.shape[0]
+    query_width = w_query.shape[1] // layers
+    pair_width = 2 * (w_key.shape[1] // layers)
+    state_width = w_state_in.shape[1] // layers
+    width = query_width + pair_width + state_width
+    groups, states, group_width = (in_re.shape[0] // layers, in_re.shape[1], in_re.shape[2])
+    kinds = state_width // LANES
+    lanes = groups // kinds * states
+    height, out_width = w_attn_out.shape
+    half = HEAD // 2
+    frequency = rotary_base ** (-(np.arange(half) * 2.0 / HEAD))
+    frequency = np.tile(frequency, LANES // half)[None, :]
+    within = np.arange(rows)[:, None] * frequency
+    across = (np.arange(layers * PLANE) * rows)[:, None] * frequency
+    tables = [np.cos(within), np.sin(within), np.cos(across), np.sin(across)]
+    tables = [jnp.asarray(t, jnp.float32) for t in tables]
+    anywhere = pl.BlockSpec(memory_space=pl.ANY)
+    vmem = pl.BlockSpec(memory_space=pltpu.VMEM)
+    smem = pl.BlockSpec(memory_space=pltpu.SMEM)
+    dma = pltpu.SemaphoreType.DMA
+    low, full = (jnp.bfloat16, jnp.float32)
+    piece = pltpu.VMEM((layers, half_rows, PLANE * out_width), low)
+
+    def halved(matrix):
+        return matrix.reshape(2, matrix.shape[0] // 2, matrix.shape[1])
+
+    return pl.pallas_call(
+        whole_kernel,
+        out_shape=jax.ShapeDtypeStruct((half_rows, model), low),
+        in_specs=[anywhere] * 11 + [vmem] * 9 + [smem] * 2,
+        out_specs=vmem,
+        scratch_shapes=[
+            pltpu.VMEM((2, 2, depth // 2, w_key.shape[1]), low),
+            pltpu.VMEM((layers, 2, depth // 2, pair_width), low),
+            pltpu.VMEM((layers, PLANE, 2, depth // 2, width), low),
+            pltpu.VMEM((layers, CORES, half_rows, model), low),
+            pltpu.VMEM((rows, model), low),
+            pltpu.VMEM((groups, states, group_width), full),
+            pltpu.VMEM((groups, states, group_width), full),
+            pltpu.VMEM((groups, group_width, states), full),
+            pltpu.VMEM((groups, group_width, states), full),
+            pltpu.VMEM((kinds, 2 * LANES, 2 * lanes), low),
+            pltpu.VMEM((kinds, 2 * LANES, 2 * lanes), low),
+            pltpu.VMEM((4, SUB, groups * states), full),
+            pltpu.VMEM((layers, rows, query_width), low),
+            pltpu.VMEM((layers, rows, pair_width), low),
+            pltpu.VMEM((layers + 1, rows, pair_width), low),
+            pltpu.VMEM((layers, rows, state_width), low),
+            pltpu.VMEM((layers, kinds, rows, 2 * lanes), full),
+            pltpu.VMEM((layers, kinds, SUB, 2 * lanes), full),
+            pltpu.VMEM((PLANE, layers, kinds, 1, 2 * lanes), full),
+            pltpu.VMEM((layers * PLANE, kinds, 1, 2 * lanes), full),
+            pltpu.VMEM((layers, 2, layers, rows, query_width), low),
+            pltpu.VMEM((2, PLANE, 2, height // 2, out_width), low),
+            pltpu.VMEM((CORES, layers, half_rows, PLANE * out_width), low),
+            piece, piece, piece,
+            dma((11,)), dma((layers, 3)), dma((layers, 3)),
+            dma((2, layers)), dma((2, layers)), dma((2, layers)), dma((2, layers)),
+            dma((layers, 2, 3)), dma((layers, 2, 3)), dma((layers,)), dma((layers + 1,)),
+            dma((PLANE - 1, layers)), dma((PLANE - 1, layers)),
+            dma((2, 2, layers)), dma((2, 2, layers)), dma((2, 2, 3)), dma((2, 2, 3)),
+            dma((2,)), dma((layers,)), dma((layers,)),
+        ],
+        compiler_params=pltpu.CompilerParams(
+            collective_id=0, has_side_effects=True, vmem_limit_bytes=60 * 2**20
+        ),
+    )(
+        tokens.reshape(CORES, half_rows, model), halved(w_query), halved(w_key), halved(w_value),
+        halved(w_state_in), in_re, in_im, out_re, out_im, halved(w_attn_out),
+        halved(w_state_out), norm_gain.reshape(1, -1), out_gain.reshape(1, -1), decay_rate,
+        rotation, skip_gain.reshape(1, -1), *tables, log_step, sink_logit,
+    )
+
+
+def suits(mesh, shapes):
+    size, cores = (mesh.shape["sp"], mesh.shape["tp"])
+    layers = size // PLANE
+    query_width, key_width, state_width = (shapes[at][1] // cores for at in (2, 3, 5))
+    return (
+        size % PLANE == 0
+        and layers > 1
+        and layers % 2 == 0
+        and cores == CORES
+        and shapes[0][0] // size == WINDOW
+        and key_width == layers * HEAD
+        and state_width == query_width
+        and query_width % (layers * LANES) == 0
+    )
+
+
 def solution(mesh):
+    def run(*arrays):
+        chosen = body if suits(mesh, [array.shape for array in arrays]) else whole_weights_body
+        return sharded(mesh, chosen)(*arrays)
+
+    return run
+
+
+def sharded(mesh, chosen):
     return jax.shard_map(
-        body,
+        chosen,
         mesh=mesh,
         in_specs=(
             P("sp", None),

time: 658 us -> 162 us (0.25)
  waiting for transfers between devices: 487 us -> 0 us
  Pallas kernels: 19.6 us -> 155 us
  local copies, waits for them, and re-layouts: 63.1 us -> 6.88 us
  matrix products: 28.4 us -> 0 us
  starting transfers between devices: 24.3 us -> 0 us
  other arithmetic: 20.1 us -> 0 us
  between operations: 14.1 us -> 0.01 us
    all_gather x6 -> x0, waiting for transfers between devices: 472 us -> none  [the longest x1 120 us: body(): lax.all_gather(w_state_out, 'sp', axis=1, tiled=True)]
    pallas_call x2 -> x1, Pallas kernels: 19.6 us -> 155 us  [body(): pl.pallas_call(whole_kernel, out_shape=jax.ShapeDtypeStruct((half_rows, m...]
    broadcast_in_dim x15 -> x0, local copies, waits for them, and re-layouts: 32.3 us -> none  [block_diagonal(): jnp.where(same, part[:, :, :, None, :], 0.0)]
    dot_general x8 -> x0, matrix products: 28.4 us -> none  [the longest x4 17 us: add_pieces(): lax.dot_general(normed_cols, weight_piece, (((0,), (0,)), ((), ())), pref...]
    ppermute x6 -> x0, starting transfers between devices: 24 us -> none  [passed_along(): return lax.ppermute(value, axis, pairs)]
    reshape x12 -> x0, local copies, waits for them, and re-layouts: 15.9 us -> none  [the longest x8 11.5 us: carried_state(): power_re, power_im = (power_re.reshape(shape), power_im.reshape(shape))]
    another operation x18 -> x0, local copies, waits for them, and re-layouts: 7.73 us -> none  [the longest x9 6.2 us: state_tables(): chunk_re = jnp.stack([p[0].reshape(groups * states) for p in chunk_powers])]
    unnamed x56 -> x5, local copies, waits for them, and re-layouts: 0.12 us -> 6.88 us
  transfers between devices with their start and end apart: 13 -> 0, of which waited for: 10 -> 0; matrix products, arithmetic and copies ran while one was open for 16% -> 0% of each run, Pallas kernels for 3% -> 0%
where the time goes in v2:
time: 162 us
  Pallas kernels  155 us (96%)
  local copies, waits for them, and re-layouts  6.88 us (4%)
    pallas_call x1, Pallas kernels, body(): pl.pallas_call(whole_kernel, out_shape=jax.ShapeDtypeStruct((half_rows, m...  155 us
    unnamed x5, local copies, waits for them, and re-layouts  6.88 us

profile of v2, /device:TPU:0, one launch (start us, length us, event | category | flops | bytes accessed | tf_op | source)
XLA Modules:
  0.0 161.7 jit_solution(3346473583433369800)
XLA Ops:
  0.0 0.0 copy-start
  0.0 3.1 %copy.23.in_re_ref = f32[64,64,16]{2,1,0:T(8,128)} copy(f32[64,64,16]{1,2,0:T(8,128)} %param.32) | data formatting | bytes 524288 | tf_op args[10]
  3.1 0.0 copy-done
  3.1 1.9 %copy.24.in_im_ref = f32[64,64,16]{2,1,0:T(8,128)} copy(f32[64,64,16]{1,2,0:T(8,128)S(1)} %copy-done) | data formatting | bytes 524288 | tf_op args[11]
  5.0 154.9 %shard_map.208 = bf16[64,4096]{1,0:T(8,128)(2,1)} custom-call(bf16[2,64,4096]{2,1,0:T(8,128)(2,1)} %bitcast.10, bf16[2,128,1024]{2,1,0:T(8,128)(2,1)} %bitcast.11, bf16[2,128,256]{2,1,0:T(8,128)(2,1)} %bitcast.15, bf16[2,128,256]{2,1,0:T(8,128)(2,1)} %bitcast.16, bf16[2,128,1024]{2,1,0:T(8,128)(2,1)} %bitcast.12, f32[64,64,16]{2,1,0:T(8,128)} %copy.23.in_re_ref, ...), custom_call_target="tpu_custom_call" | custom-call | tf_op jit(solution)/shard_map/pallas_call | solution.py:1204
  159.9 1.9 %copy.26 = bf16[64,4096]{1,0:T(8,128)(2,1)} copy(bf16[64,4096]{1,0:T(8,128)(2,1)} %shard_map.208) | data formatting | bytes 1048576
Async XLA Ops:
  0.0 3.1 %copy-start = (f32[64,64,16]{1,2,0:T(8,128)S(1)}, f32[64,64,16]{1,2,0:T(8,128)}, u32[]{:S(2)}) copy-start(f32[64,64,16]{1,2,0:T(8,128)} %param.33) | copy-start | bytes 786436

commit v3 on v2

--- a/solution.py
+++ b/solution.py
@@ -535,24 +535,24 @@
             ).wait_send()
 
 
+def plane_halves(halves, slots, layer, spot, send_sems, recv_sems, half):
+    beside, above = plane_neighbours(spot)
+    return [
+        remote(
+            halves.at[half], slots.at[spot, half], send_sems.at[0, half],
+            recv_sems.at[0, half], {"sp": layer * PLANE + beside},
+        ),
+        remote(
+            halves.at[1 - half], slots.at[spot, 1 - half], send_sems.at[1, 1 - half],
+            recv_sems.at[1, 1 - half], {"sp": layer * PLANE + above},
+        ),
+    ]
+
+
 def plane_first(halves, slots, layer, spot, send_sems, recv_sems):
-    beside, above = plane_neighbours(spot)
-    copies = []
     for half in (0, 1):
-        copies.append(
-            remote(
-                halves.at[half], slots.at[spot, half], send_sems.at[0, half],
-                recv_sems.at[0, half], {"sp": layer * PLANE + beside},
-            )
-        )
-        copies.append(
-            remote(
-                halves.at[1 - half], slots.at[spot, 1 - half], send_sems.at[1, 1 - half],
-                recv_sems.at[1, 1 - half], {"sp": layer * PLANE + above},
-            )
-        )
-    for copy in copies:
-        copy.start()
+        for copy in plane_halves(halves, slots, layer, spot, send_sems, recv_sems, half):
+            copy.start()
 
 
 def plane_pass(slots, layer, spot, send_sems, recv_sems):
@@ -592,7 +592,7 @@
     layer, rows, decay_ref, rotation_ref, step_ref, in_re_ref, in_im_ref, out_re_ref, out_im_ref,
     drive, read, powers,
 ):
-    groups, states, group_width = in_re_ref.shape
+    groups, group_width, states = in_re_ref.shape
     kinds, _, width2 = drive.shape
     per = groups // kinds
     width = per * states
@@ -633,8 +633,8 @@
         lanes = slice(kind * width, (kind + 1) * width)
         f_re, f_im = (factor_re[:, lanes], factor_im[:, lanes])
         own = range(kind * per, (kind + 1) * per)
-        m_re = spread([jnp.transpose(in_re_ref[at]) for at in own])
-        m_im = spread([jnp.transpose(in_im_ref[at]) for at in own])
+        m_re = spread([in_re_ref[at] for at in own])
+        m_im = spread([in_im_ref[at] for at in own])
         for part, value in ((0, f_re * m_re - f_im * m_im), (1, f_re * m_im + f_im * m_re)):
             high, low = split_pair(jnp.where(same, value, 0.0))
             columns = slice(part * width, (part + 1) * width)
@@ -833,10 +833,11 @@
     out_ref,
     key_value, packed, weights, held, normed, in_re, in_im, out_re, out_im, drive, read, powers,
     queries, pairs, before, inputs, states, carries, ends, priors,
-    mixers, matrices, partial, arrived, summed, pieces,
+    mixers, matrices, total, partial, arrived, summed, pieces,
     load_sem, far_send, far_recv, line_send, line_recv, part_send, part_recv,
     side_send, side_recv, halo_send, halo_recv, end_send, end_recv,
-    mixer_send, mixer_recv, matrix_send, matrix_recv, half_sem, piece_send, piece_recv,
+    mixer_send, mixer_recv, matrix_send, matrix_recv, half_send, half_recv,
+    piece_send, piece_recv,
 ):
     layers = held.shape[0]
     rows = pairs.shape[1]
@@ -873,39 +874,54 @@
     ]
     for copy in loads + own_weights + [own_tokens] + table_loads + matrix_loads:
         copy.start()
-    greet(layers, layer, spot, core)
-    far = []
-    for ahead in range(1, layers):
-        other = lax.rem(layer + ahead, layers)
-        for source, wide, to, at in spans:
-            far.append(
-                remote(
-                    source.at[:, :, pl.ds(pl.multiple_of(other * wide, wide), wide)],
-                    weights.at[layer, spot, :, :, pl.ds(to, wide)],
-                    far_send.at[ahead, at], far_recv.at[ahead, at], {"sp": other * PLANE + spot},
-                )
-            )
-            far[-1].start()
     for copy in loads:
         copy.wait()
     for at in range(layers):
         head = slice(at * HEAD, (at + 1) * HEAD)
         packed[at] = jnp.concatenate([key_value[0, :, :, head], key_value[1, :, :, head]], axis=-1)
     middle = pl.ds(query_width, pair_width)
-    for ahead in range(1, layers):
-        other = lax.rem(layer + ahead, layers)
-        far.append(
+    weights[layer, spot, :, :, query_width : query_width + pair_width] = packed[layer]
+    greet(layers, layer, spot, core)
+
+    def far_copies(way, hop):
+        other = layer + hop if way == 0 else layer - hop
+        device = {"sp": other * PLANE + spot}
+        sources = [
+            (source.at[:, :, pl.ds(pl.multiple_of(other * wide, wide), wide)], pl.ds(to, wide))
+            for source, wide, to, _ in spans
+        ] + [(packed.at[other], middle)]
+        return [
             remote(
-                packed.at[other], weights.at[layer, spot, :, :, middle],
-                far_send.at[ahead, 1], far_recv.at[ahead, 1], {"sp": other * PLANE + spot},
+                source, weights.at[layer, spot, :, :, columns],
+                far_send.at[way, hop, at], far_recv.at[way, hop, at], device,
             )
-        )
-        far[-1].start()
-    weights[layer, spot, :, :, query_width : query_width + pair_width] = packed[layer]
+            for at, (source, columns) in enumerate(sources)
+        ]
+
+    def each_far(action):
+        for hop in range(1, layers):
+            for way, there in ((0, layer + hop <= layers - 1), (1, layer - hop >= 0)):
+
+                @pl.when(there)
+                def _():
+                    for copy in far_copies(way, hop):
+                        action(copy)
+
+    each_far(lambda copy: copy.start())
     half_held = held.at[:, core]
     line_first(layers, layer, spot, tokens_ref.at[core], half_held, line_send, line_recv)
     for copy in own_weights:
         copy.wait()
+
+    below, above = (layer, layers - 1 - layer)
+    least = jnp.minimum(below, above)
+
+    def arrival(at):
+        paired = at <= 2 * least
+        hop = jnp.where(paired, lax.div(at + 1, 2), at - least)
+        way = jnp.where(paired, lax.rem(at, 2), jnp.where(below > above, 0, 1))
+        return (jnp.where(way == 0, layer - hop, layer + hop), hop, way)
+
     plane_first(
         weights.at[layer, spot], weights.at[layer], layer, spot, side_send.at[0], side_recv.at[0]
     )
@@ -916,43 +932,36 @@
         drive, read, powers,
     )
     before[0] = jnp.zeros(before.shape[1:], before.dtype)
+    plane_pass(weights.at[layer], layer, spot, side_send.at[0], side_recv.at[0])
 
     def to_partner(way, hop, block):
         remote(
             block, block, part_send.at[way, hop - 1], part_recv.at[way, hop - 1], {"tp": 1 - core}
         ).start()
 
-    for ahead in range(layers):
-        origin = lax.rem(layer + layers - ahead, layers)
-        if ahead > 0:
-            for at, (to, wide) in enumerate(
-                ((0, query_width), (query_width, pair_width),
-                 (query_width + pair_width, state_width))
-            ):
-                block = weights.at[origin, spot, :, :, pl.ds(to, wide)]
-                remote(
-                    block, block, far_send.at[ahead, at], far_recv.at[ahead, at], {"sp": 0}
-                ).wait_recv()
-            plane_first(
-                weights.at[origin, spot], weights.at[origin], layer, spot,
-                side_send.at[ahead], side_recv.at[ahead],
-            )
-        plane_pass(weights.at[origin], layer, spot, side_send.at[ahead], side_recv.at[ahead])
+    for at in range(1, layers):
+        origin, hop, way = arrival(jnp.int32(at))
+        for part, (to, wide) in enumerate(
+            ((0, query_width), (query_width + pair_width, state_width), (query_width, pair_width))
+        ):
+            block = weights.at[origin, spot, :, :, pl.ds(to, wide)]
+            remote(
+                block, block, far_send.at[0, 0, 0], far_recv.at[way, hop, part], {"sp": 0}
+            ).wait_recv()
+        plane_first(
+            weights.at[origin, spot], weights.at[origin], layer, spot,
+            side_send.at[at], side_recv.at[at],
+        )
+        plane_pass(weights.at[origin], layer, spot, side_send.at[at], side_recv.at[at])
+    line_pass(layers, layer, spot, 1, half_held, line_send, line_recv, to_partner)
+    own_tokens.wait()
     for copy in matrix_loads:
         copy.wait()
-    plane_first(
-        matrices.at[0, spot], matrices.at[0], layer, spot, matrix_send.at[0], matrix_recv.at[0]
-    )
-    line_pass(layers, layer, spot, 1, half_held, line_send, line_recv, to_partner)
-    own_tokens.wait()
-    for ahead in range(layers):
-        origin = lax.rem(layer + layers - ahead, layers)
-        plane_landed(weights.at[origin], spot, side_send.at[ahead], side_recv.at[ahead])
-    for copy in far:
-        copy.wait_send()
-
-    below, above = (layer, layers - 1 - layer)
-    least = jnp.minimum(below, above)
+    for at in range(layers):
+        origin = layer if at == 0 else arrival(jnp.int32(at))[0]
+        plane_landed(weights.at[origin], spot, side_send.at[at], side_recv.at[at])
+    each_far(lambda copy: copy.wait_send())
+
     behind = layer * PLANE + lax.rem(spot + 1, PLANE)
     late = lax.div(spot, PLANE - 1)
 
@@ -976,11 +985,7 @@
 
     @pl.loop(0, layers)
     def _(at):
-        paired = at <= 2 * least
-        hop = jnp.where(paired, lax.div(at + 1, 2), at - least)
-        way = jnp.where(paired, lax.rem(at + 1, 2), jnp.where(below > above, 1, 0))
-        way = 1 - way
-        block = jnp.where(at == 0, layer, jnp.where(way == 0, layer - hop, layer + hop))
+        block, hop, way = arrival(at)
 
         @pl.when(at > 0)
         def _():
@@ -1020,6 +1025,16 @@
         scan_block(block, spot, inputs, drive, powers, states, carries, ends)
         for peer in range(PLANE - 1):
             tell(block, peer).start()
+
+        kind, half = (lax.div(at, 2), lax.rem(at, 2))
+
+        @pl.when(kind < 2)
+        def _():
+            for copy in plane_halves(
+                matrices.at[kind, spot], matrices.at[kind], layer, spot, matrix_send.at[kind],
+                matrix_recv.at[kind], half,
+            ):
+                copy.start()
 
         @pl.when((spot > 0) | (block == 0) | ((at > 0) & (way == 1)))
         def _():
@@ -1043,38 +1058,145 @@
     def _():
         arrive(layers)
 
-    for kind in (0, 1):
-        if kind == 1:
-            for block in range(layers):
-                for peer in range(PLANE - 1):
-                    tell(block, peer).wait()
-            find_priors(ends, powers, priors)
-
-            @pl.loop(0, layers)
-            def _(block):
-                read_block(
-                    block, layer, spot, inputs, states, carries, priors, powers, read, skip_ref,
-                    mixers.at[layer, 1, block],
-                )
-
+    def mixers_first(kind):
         line_first(
             layers, layer, spot, mixers.at[layer, kind], mixers.at[:, kind],
             mixer_send.at[kind], mixer_recv.at[kind],
         )
+
+    mixers_first(0)
     plane_pass(matrices.at[0], layer, spot, matrix_send.at[0], matrix_recv.at[0])
-    plane_first(
-        matrices.at[1, spot], matrices.at[1], layer, spot, matrix_send.at[1], matrix_recv.at[1]
-    )
-    for hop in range(1, layers):
-        for kind in (0, 1):
-            line_pass(
-                layers, layer, spot, hop, mixers.at[:, kind], mixer_send.at[kind],
-                mixer_recv.at[kind],
-            )
-        if hop == 1:
-            plane_pass(matrices.at[1], layer, spot, matrix_send.at[1], matrix_recv.at[1])
+    for block in range(layers):
+        for peer in range(PLANE - 1):
+            tell(block, peer).wait()
+    find_priors(ends, powers, priors)
+
+    @pl.loop(0, layers)
+    def _(block):
+        read_block(
+            block, layer, spot, inputs, states, carries, priors, powers, read, skip_ref,
+            mixers.at[layer, 1, block],
+        )
+
+    mixers_first(1)
+    plane_pass(matrices.at[1], layer, spot, matrix_send.at[1], matrix_recv.at[1])
+    for kind in (0, 1):
+        line_pass(
+            layers, layer, spot, 1, mixers.at[:, kind], mixer_send.at[kind], mixer_recv.at[kind]
+        )
     for kind in (0, 1):
         plane_landed(matrices.at[kind], spot, matrix_send.at[kind], matrix_recv.at[kind])
+
+    depth = mixers.shape[-1]
+    tokens = layers * rows
+    half_depth, width = matrices.shape[3:]
+    half_rows = rows // CORES
+    per = half_depth // depth
+
+    def take(at):
+        block, hop, way = arrival(at)
+
+        @pl.when(hop > 1)
+        def _():
+            for kind in (0, 1):
+                columns = mixers.at[block, kind]
+                remote(
+                    columns, columns, mixer_send.at[kind, 0, 0],
+                    mixer_recv.at[kind, way, hop - 1], {"sp": 0},
+                ).wait_recv()
+                onward = jnp.where(way == 0, layer < layers - 1, layer > 0)
+
+                @pl.when(onward & (hop < layers - 1))
+                def _():
+                    remote(
+                        columns, columns, mixer_send.at[kind, way, hop],
+                        mixer_recv.at[kind, way, hop],
+                        {"sp": (layer + 1 - 2 * way) * PLANE + spot},
+                    ).start()
+
+        return block
+
+    def product(block, column):
+        low = pl.ds(pl.multiple_of(lax.rem(block, per) * depth, depth), depth)
+        return sum(
+            jnp.dot(
+                mixers[block, kind].reshape(tokens, depth),
+                matrices[kind, column, lax.div(block, per), low, :],
+                preferred_element_type=jnp.float32,
+            )
+            for kind in (0, 1)
+        )
+
+    @pl.loop(0, layers - 1)
+    def _(at):
+        block = take(at)
+        for column in range(PLANE):
+            value = product(block, column)
+
+            @pl.when(at == 0)
+            def _():
+                total[column] = value
+
+            @pl.when(at > 0)
+            def _():
+                total[column] += value
+
+    last = take(jnp.int32(layers - 1))
+
+    def swap(column):
+        return remote(
+            partial.at[column, 1 - core], arrived.at[column], half_send.at[column],
+            half_recv.at[column], {"tp": 1 - core},
+        )
+
+    def each_piece(column, action):
+        for hop in range(layers - 1, 0, -1):
+            for way, there in ((0, layer + hop <= layers - 1), (1, layer - hop >= 0)):
+
+                @pl.when(there)
+                def _():
+                    other = layer + hop if way == 0 else layer - hop
+                    action(
+                        remote(
+                            summed.at[column, other], pieces.at[column, layer],
+                            piece_send.at[column, way, hop], piece_recv.at[column, way, hop],
+                            {"sp": other * PLANE + spot},
+                        )
+                    )
+
+    def each_landing(column):
+        for hop in range(1, layers):
+            for way, there in ((0, layer - hop >= 0), (1, layer + hop <= layers - 1)):
+
+                @pl.when(there)
+                def _():
+                    other = layer - hop if way == 0 else layer + hop
+                    piece = pieces.at[column, other]
+                    remote(
+                        piece, piece, piece_send.at[0, 0, 0], piece_recv.at[column, way, hop],
+                        {"sp": 0},
+                    ).wait_recv()
+
+    def send_column(column):
+        swap(column).wait_recv()
+        for at in range(layers):
+            summed[column, at] = (
+                partial[column, core, at].astype(jnp.float32)
+                + arrived[column, at].astype(jnp.float32)
+            ).astype(jnp.bfloat16)
+        each_piece(column, lambda copy: copy.start())
+        pieces[column, layer] = summed[column, layer]
+
+    for column in range(PLANE):
+        value = total[column] + product(last, column)
+        value = value.astype(jnp.bfloat16).reshape(layers, CORES, half_rows, width)
+        for half in range(CORES):
+            partial[column, half] = value[:, half]
+        swap(column).start()
+        if column > 0:
+            send_column(column - 1)
+    send_column(PLANE - 1)
+    for kind in (0, 1):
         line_drain(
             layers, layer, mixers.at[layer, kind], mixers.at[:, kind], mixer_send.at[kind],
             mixer_recv.at[kind],
@@ -1093,63 +1215,24 @@
 
     for block in range(layers):
         hand_on(block).wait_send()
-
-    depth = mixers.shape[-1]
-    tokens = layers * rows
-    half_depth, width = matrices.shape[3:]
-    half_rows = rows // CORES
-
-    @pl.loop(0, PLANE)
-    def _(block):
-        total = None
+    for column in range(PLANE):
+        each_landing(column)
+    for column in range(PLANE):
+        swap(column).wait_send()
+        each_piece(column, lambda copy: copy.wait_send())
+    squares = jnp.zeros((half_rows, 1), jnp.float32)
+    for column in range(PLANE):
         for at in range(layers):
-            for kind in (0, 1):
-                low = at * depth
-                piece = jnp.dot(
-                    mixers[at, kind].reshape(tokens, depth),
-                    matrices[kind, block, low // half_depth, pl.ds(low % half_depth, depth), :],
-                    preferred_element_type=jnp.float32,
-                )
-                total = piece if total is None else total + piece
-        rounded = total.astype(jnp.bfloat16).reshape(layers, CORES, half_rows, width)
-        columns = pl.ds(pl.multiple_of(block * width, width), width)
-        for half in range(CORES):
-            partial[half, :, :, columns] = rounded[:, half]
-
-    swap = remote(
-        partial.at[1 - core], arrived, half_sem.at[0], half_sem.at[1], {"tp": 1 - core}
-    )
-    swap.start()
-    swap.wait()
+            value = pieces[column, at].astype(jnp.float32)
+            squares = squares + jnp.sum(value * value, axis=-1, keepdims=True)
+    scale = lax.rsqrt(squares / (layers * PLANE * width) + epsilon)
     for at in range(layers):
-        summed[at] = (
-            partial[core, at].astype(jnp.float32) + arrived[at].astype(jnp.float32)
-        ).astype(jnp.bfloat16)
-    copies = []
-    for ahead in range(1, layers):
-        other = lax.rem(layer + ahead, layers)
-        copies.append(
-            remote(
-                summed.at[other], pieces.at[layer], piece_send.at[ahead], piece_recv.at[ahead],
-                {"sp": other * PLANE + spot},
-            )
-        )
-    for copy in copies:
-        copy.start()
-    pieces[layer] = summed[layer]
-    for copy in copies:
-        copy.wait()
-    squares = jnp.zeros((half_rows, 1), jnp.float32)
-    span = pieces.shape[-1]
-    for at in range(layers):
-        value = pieces[at].astype(jnp.float32)
-        squares = squares + jnp.sum(value * value, axis=-1, keepdims=True)
-    scale = lax.rsqrt(squares / (layers * span) + epsilon)
-    for at in range(layers):
-        columns = slice(at * span, (at + 1) * span)
-        out_ref[:, columns] = (
-            pieces[at].astype(jnp.float32) * scale * out_gain_ref[:, columns]
-        ).astype(jnp.bfloat16)
+        for column in range(PLANE):
+            low = (at * PLANE + column) * width
+            columns = slice(low, low + width)
+            out_ref[:, columns] = (
+                pieces[column, at].astype(jnp.float32) * scale * out_gain_ref[:, columns]
+            ).astype(jnp.bfloat16)
 
 
 def body(
@@ -1196,7 +1279,7 @@
     smem = pl.BlockSpec(memory_space=pltpu.SMEM)
     dma = pltpu.SemaphoreType.DMA
     low, full = (jnp.bfloat16, jnp.float32)
-    piece = pltpu.VMEM((layers, half_rows, PLANE * out_width), low)
+    piece = pltpu.VMEM((PLANE, layers, half_rows, out_width), low)
 
     def halved(matrix):
         return matrix.reshape(2, matrix.shape[0] // 2, matrix.shape[1])
@@ -1212,8 +1295,8 @@
             pltpu.VMEM((layers, PLANE, 2, depth // 2, width), low),
             pltpu.VMEM((layers, CORES, half_rows, model), low),
             pltpu.VMEM((rows, model), low),
-            pltpu.VMEM((groups, states, group_width), full),
-            pltpu.VMEM((groups, states, group_width), full),
+            pltpu.VMEM((groups, group_width, states), full),
+            pltpu.VMEM((groups, group_width, states), full),
             pltpu.VMEM((groups, group_width, states), full),
             pltpu.VMEM((groups, group_width, states), full),
             pltpu.VMEM((kinds, 2 * LANES, 2 * lanes), low),
@@ -1229,21 +1312,22 @@
             pltpu.VMEM((layers * PLANE, kinds, 1, 2 * lanes), full),
             pltpu.VMEM((layers, 2, layers, rows, query_width), low),
             pltpu.VMEM((2, PLANE, 2, height // 2, out_width), low),
-            pltpu.VMEM((CORES, layers, half_rows, PLANE * out_width), low),
+            pltpu.VMEM((PLANE, layers * rows, out_width), full),
+            pltpu.VMEM((PLANE, CORES, layers, half_rows, out_width), low),
             piece, piece, piece,
-            dma((11,)), dma((layers, 3)), dma((layers, 3)),
+            dma((11,)), dma((2, layers, 3)), dma((2, layers, 3)),
             dma((2, layers)), dma((2, layers)), dma((2, layers)), dma((2, layers)),
             dma((layers, 2, 3)), dma((layers, 2, 3)), dma((layers,)), dma((layers + 1,)),
             dma((PLANE - 1, layers)), dma((PLANE - 1, layers)),
             dma((2, 2, layers)), dma((2, 2, layers)), dma((2, 2, 3)), dma((2, 2, 3)),
-            dma((2,)), dma((layers,)), dma((layers,)),
+            dma((PLANE,)), dma((PLANE,)), dma((PLANE, 2, layers)), dma((PLANE, 2, layers)),
         ],
         compiler_params=pltpu.CompilerParams(
             collective_id=0, has_side_effects=True, vmem_limit_bytes=60 * 2**20
         ),
     )(
         tokens.reshape(CORES, half_rows, model), halved(w_query), halved(w_key), halved(w_value),
-        halved(w_state_in), in_re, in_im, out_re, out_im, halved(w_attn_out),
+        halved(w_state_in), jnp.swapaxes(in_re, 1, 2), jnp.swapaxes(in_im, 1, 2), out_re, out_im, halved(w_attn_out),
         halved(w_state_out), norm_gain.reshape(1, -1), out_gain.reshape(1, -1), decay_rate,
         rotation, skip_gain.reshape(1, -1), *tables, log_step, sink_logit,
     )
@@ -1255,8 +1339,7 @@
     query_width, key_width, state_width = (shapes[at][1] // cores for at in (2, 3, 5))
     return (
         size % PLANE == 0
-        and layers > 1
-        and layers % 2 == 0
+        and layers % 4 == 0
         and cores == CORES
         and shapes[0][0] // size == WINDOW
         and key_width == layers * HEAD

time: 162 us -> 142 us (0.88)
  Pallas kernels: 155 us -> 140 us
  local copies, waits for them, and re-layouts: 6.88 us -> 1.87 us
    pallas_call x1, Pallas kernels: 155 us -> 140 us  [body(): pl.pallas_call(whole_kernel, out_shape=jax.ShapeDtypeStruct((half_rows, m...]
    unnamed x5 -> x1, local copies, waits for them, and re-layouts: 6.88 us -> 1.87 us
where the time goes in v3:
time: 142 us; the launch traced here: 141 us
  Pallas kernels  140 us (99%)
  local copies, waits for them, and re-layouts  1.87 us (1%)
    pallas_call x1, Pallas kernels, body(): pl.pallas_call(whole_kernel, out_shape=jax.ShapeDtypeStruct((half_rows, m...  140 us

profile of v3, /device:TPU:0, one launch (start us, length us, event | category | flops | bytes accessed | tf_op | source)
XLA Modules:
  0.0 141.4 jit_solution(17430447251369499097)
XLA Ops:
  0.0 139.6 %shard_map.208 = bf16[64,4096]{1,0:T(8,128)(2,1)} custom-call(bf16[2,64,4096]{2,1,0:T(8,128)(2,1)} %bitcast.12, bf16[2,128,1024]{2,1,0:T(8,128)(2,1)} %bitcast.13, bf16[2,128,256]{2,1,0:T(8,128)(2,1)} %bitcast.19, bf16[2,128,256]{2,1,0:T(8,128)(2,1)} %bitcast.20, bf16[2,128,1024]{2,1,0:T(8,128)(2,1)} %bitcast.14, f32[64,16,64]{2,1,0:T(8,128)} %bitcast.15, ...), custom_call_target="tpu_custom_call" | custom-call | tf_op jit(solution)/shard_map/pallas_call | solution.py:1287
  139.6 1.9 %copy.24 = bf16[64,4096]{1,0:T(8,128)(2,1)} copy(bf16[64,4096]{1,0:T(8,128)(2,1)} %shard_map.208) | data formatting | bytes 1048576

commit v4 on v3

--- a/solution.py
+++ b/solution.py
@@ -431,6 +431,7 @@
 SIDE = 2
 PLANE = SIDE * SIDE
 CORES = 2
+CHUNKS = 2
 LANES = 128
 MESH = pl.DeviceIdType.MESH
 
@@ -650,23 +651,24 @@
 
 
 def normalise(block, held, gain_ref, normed):
-    _, parts, part_rows, model = held.shape
+    _, parts, chunks, part_rows, model = held.shape
     tall = 16
     per = part_rows // tall
 
-    @pl.loop(0, parts * per)
+    @pl.loop(0, parts * chunks * per)
     def _(at):
         value = held[
-            block, at // per, pl.ds(pl.multiple_of((at % per) * tall, tall), tall), :
+            block, at // (chunks * per), (at // per) % chunks,
+            pl.ds(pl.multiple_of((at % per) * tall, tall), tall), :,
         ].astype(jnp.float32)
         scale = lax.rsqrt(jnp.sum(value * value, axis=-1, keepdims=True) / model + epsilon)
-        normed[pl.ds(pl.multiple_of(at * tall, tall), tall), :] = (
+        normed[block, pl.ds(pl.multiple_of(at * tall, tall), tall), :] = (
             value * scale * gain_ref[...]
         ).astype(jnp.bfloat16)
 
 
 def project_block(block, spot, normed, weights, tables, queries, pairs, inputs):
-    rows, model = normed.shape
+    rows = normed.shape[1]
     layers = weights.shape[0]
     depth = weights.shape[2] * weights.shape[3]
     query_width, pair_width = (queries.shape[-1], pairs.shape[-1])
@@ -684,7 +686,7 @@
     total = None
     for at in range(layers * PLANE):
         piece = jnp.dot(
-            normed[:, at * depth : (at + 1) * depth],
+            normed[block, :, at * depth : (at + 1) * depth],
             weights[at // PLANE, at % PLANE].reshape(depth, weights.shape[-1]),
             preferred_element_type=jnp.float32,
         )
@@ -834,7 +836,7 @@
     key_value, packed, weights, held, normed, in_re, in_im, out_re, out_im, drive, read, powers,
     queries, pairs, before, inputs, states, carries, ends, priors,
     mixers, matrices, total, partial, arrived, summed, pieces,
-    load_sem, far_send, far_recv, line_send, line_recv, part_send, part_recv,
+    load_sem, pack_sem, far_send, far_recv, line_send, line_recv, part_send, part_recv,
     side_send, side_recv, halo_send, halo_recv, end_send, end_recv,
     mixer_send, mixer_recv, matrix_send, matrix_recv, half_send, half_recv,
     piece_send, piece_recv,
@@ -851,16 +853,20 @@
         pltpu.make_async_copy(value_ref, key_value.at[1], load_sem.at[1]),
     ]
     spans = (
-        (query_ref, query_width, 0, 0),
-        (state_ref, state_width, query_width + pair_width, 2),
-    )
-    own_weights = [
-        pltpu.make_async_copy(
-            source.at[:, :, pl.ds(pl.multiple_of(layer * wide, wide), wide)],
-            weights.at[layer, spot, :, :, pl.ds(to, wide)], load_sem.at[2 + at],
-        )
-        for source, wide, to, at in spans
-    ]
+        (query_ref, query_width, 0),
+        (state_ref, state_width, query_width + pair_width),
+    )
+    def loaded(block, target, at):
+        return [
+            pltpu.make_async_copy(
+                source.at[:, :, pl.ds(pl.multiple_of(block * wide, wide), wide)],
+                target.at[:, :, pl.ds(to, wide)], pack_sem.at[at, part],
+            )
+            for part, (source, wide, to) in enumerate(spans)
+        ]
+
+    own_weights = loaded(layer, weights.at[layer, spot], layers)
+    far_loads = [copy for at in range(layers) for copy in loaded(at, packed.at[at], at)]
     own_tokens = pltpu.make_async_copy(tokens_ref, held.at[layer], load_sem.at[3])
     table_loads = [
         pltpu.make_async_copy(source.at[mine], target, load_sem.at[5 + at])
@@ -872,59 +878,107 @@
         pltpu.make_async_copy(source, matrices.at[kind, spot], load_sem.at[9 + kind])
         for kind, source in enumerate((attn_out_ref, state_out_ref))
     ]
-    for copy in loads + own_weights + [own_tokens] + table_loads + matrix_loads:
+    for copy in loads + own_weights + far_loads + [own_tokens] + table_loads + matrix_loads:
         copy.start()
     for copy in loads:
         copy.wait()
+    middle = slice(query_width, query_width + pair_width)
     for at in range(layers):
         head = slice(at * HEAD, (at + 1) * HEAD)
-        packed[at] = jnp.concatenate([key_value[0, :, :, head], key_value[1, :, :, head]], axis=-1)
-    middle = pl.ds(query_width, pair_width)
-    weights[layer, spot, :, :, query_width : query_width + pair_width] = packed[layer]
+        packed[at, :, :, middle] = jnp.concatenate(
+            [key_value[0, :, :, head], key_value[1, :, :, head]], axis=-1
+        )
+    weights[layer, spot, :, :, middle] = packed[layer, :, :, middle]
+    for copy in far_loads:
+        copy.wait()
     greet(layers, layer, spot, core)
-
-    def far_copies(way, hop):
-        other = layer + hop if way == 0 else layer - hop
-        device = {"sp": other * PLANE + spot}
-        sources = [
-            (source.at[:, :, pl.ds(pl.multiple_of(other * wide, wide), wide)], pl.ds(to, wide))
-            for source, wide, to, _ in spans
-        ] + [(packed.at[other], middle)]
-        return [
-            remote(
-                source, weights.at[layer, spot, :, :, columns],
-                far_send.at[way, hop, at], far_recv.at[way, hop, at], device,
-            )
-            for at, (source, columns) in enumerate(sources)
-        ]
-
-    def each_far(action):
-        for hop in range(1, layers):
-            for way, there in ((0, layer + hop <= layers - 1), (1, layer - hop >= 0)):
-
-                @pl.when(there)
-                def _():
-                    for copy in far_copies(way, hop):
-                        action(copy)
-
-    each_far(lambda copy: copy.start())
-    half_held = held.at[:, core]
-    line_first(layers, layer, spot, tokens_ref.at[core], half_held, line_send, line_recv)
-    for copy in own_weights:
-        copy.wait()
 
     below, above = (layer, layers - 1 - layer)
     least = jnp.minimum(below, above)
+    short = jnp.where(below < above, 0, 1)
 
     def arrival(at):
         paired = at <= 2 * least
         hop = jnp.where(paired, lax.div(at + 1, 2), at - least)
-        way = jnp.where(paired, lax.rem(at, 2), jnp.where(below > above, 0, 1))
+        way = jnp.where(paired & (lax.rem(at, 2) == 1), short, 1 - short)
         return (jnp.where(way == 0, layer - hop, layer + hop), hop, way)
+
+    def far_copy(way, hop):
+        other = layer + hop if way == 0 else layer - hop
+        return remote(
+            packed.at[other], weights.at[layer, spot], far_send.at[way, hop],
+            far_recv.at[way, hop], {"sp": other * PLANE + spot},
+        )
+
+    def each_far(hop, action):
+        for way, there in ((0, layer + hop <= layers - 1), (1, layer - hop >= 0)):
+
+            @pl.when(there)
+            def _():
+                action(far_copy(way, hop))
+
+    def start(copy):
+        copy.start()
+
+    each_far(1, start)
+
+    @pl.when(least > 0)
+    def _():
+        for hop in range(2, layers):
+            each_far(hop, start)
+
+    chunks = held.shape[2]
+
+    def chunk_lines(action):
+        for chunk in range(chunks):
+            action(chunk, held.at[:, core, chunk], line_send.at[chunk], line_recv.at[chunk])
+
+    for copy in own_weights:
+        copy.wait()
+
+    def part(way, hop, chunk, half):
+        block = held.at[layer + hop - 2 * hop * (1 - way), half, chunk]
+        return remote(
+            block, block, part_send.at[chunk, way, hop - 1], part_recv.at[chunk, way, hop - 1],
+            {"tp": 1 - core},
+        )
+
+    def send_tokens(side):
+        onward = 1 - side
+        for chunk in range(chunks):
+            remote(
+                tokens_ref.at[core, chunk], held.at[layer, core, chunk],
+                line_send.at[chunk, onward, 0], line_recv.at[chunk, onward, 0],
+                {"sp": (layer + 1 - 2 * onward) * PLANE + spot},
+            ).start()
+
+    def pass_tokens(way, hop):
+        block = layer + hop - 2 * hop * (1 - way)
+
+        def step(chunk, slots, send, recv):
+            half = slots.at[block]
+            remote(half, half, send.at[way, 0], recv.at[way, hop - 1], {"sp": 0}).wait_recv()
+            onward = jnp.where(way == 0, layer < layers - 1, layer > 0)
+
+            @pl.when(onward & (hop < layers - 1))
+            def _():
+                remote(
+                    half, half, send.at[way, hop], recv.at[way, hop],
+                    {"sp": (layer + 1 - 2 * way) * PLANE + spot},
+                ).start()
+
+            part(way, hop, chunk, core).start()
+
+        chunk_lines(step)
 
     plane_first(
         weights.at[layer, spot], weights.at[layer], layer, spot, side_send.at[0], side_recv.at[0]
     )
+
+    @pl.when(least == 0)
+    def _():
+        send_tokens(1 - short)
+
     for copy in table_loads:
         copy.wait()
     make_tables(
@@ -932,35 +986,69 @@
         drive, read, powers,
     )
     before[0] = jnp.zeros(before.shape[1:], before.dtype)
+    own_tokens.wait()
+    normalise(layer, held, norm_gain_ref, normed)
     plane_pass(weights.at[layer], layer, spot, side_send.at[0], side_recv.at[0])
-
-    def to_partner(way, hop, block):
-        remote(
-            block, block, part_send.at[way, hop - 1], part_recv.at[way, hop - 1], {"tp": 1 - core}
-        ).start()
 
     for at in range(1, layers):
         origin, hop, way = arrival(jnp.int32(at))
-        for part, (to, wide) in enumerate(
-            ((0, query_width), (query_width + pair_width, state_width), (query_width, pair_width))
-        ):
-            block = weights.at[origin, spot, :, :, pl.ds(to, wide)]
-            remote(
-                block, block, far_send.at[0, 0, 0], far_recv.at[way, hop, part], {"sp": 0}
-            ).wait_recv()
+        block = weights.at[origin, spot]
+        remote(block, block, far_send.at[0, 0], far_recv.at[way, hop], {"sp": 0}).wait_recv()
+
+        if at == 1:
+
+            @pl.when(least > 0)
+            def _():
+                send_tokens(short)
+
+        if at == layers - 1:
+
+            @pl.when(least > 0)
+            def _():
+                send_tokens(1 - short)
+
         plane_first(
             weights.at[origin, spot], weights.at[origin], layer, spot,
             side_send.at[at], side_recv.at[at],
         )
         plane_pass(weights.at[origin], layer, spot, side_send.at[at], side_recv.at[at])
-    line_pass(layers, layer, spot, 1, half_held, line_send, line_recv, to_partner)
-    own_tokens.wait()
+        if at == 1:
+
+            @pl.when(least == 0)
+            def _():
+                for hop in range(2, layers):
+                    each_far(hop, start)
+
     for copy in matrix_loads:
         copy.wait()
+    plane_first(
+        matrices.at[0, spot], matrices.at[0], layer, spot, matrix_send.at[0], matrix_recv.at[0]
+    )
+
+    @pl.when(least > 0)
+    def _():
+        pass_tokens(short, 1)
+
+    pass_tokens(1 - short, 1)
+
+    def landed(at):
+        block, hop, way = arrival(at)
+        for chunk in range(chunks):
+            part(way, hop, chunk, 1 - core).wait_recv()
+        normalise(block, held, norm_gain_ref, normed)
+
+    for at in range(1, layers):
+        hop = arrival(jnp.int32(at))[1]
+
+        @pl.when(hop == 1)
+        def _():
+            landed(jnp.int32(at))
+
     for at in range(layers):
         origin = layer if at == 0 else arrival(jnp.int32(at))[0]
         plane_landed(weights.at[origin], spot, side_send.at[at], side_recv.at[at])
-    each_far(lambda copy: copy.wait_send())
+    for hop in range(1, layers):
+        each_far(hop, lambda copy: copy.wait_send())
 
     behind = layer * PLANE + lax.rem(spot + 1, PLANE)
     late = lax.div(spot, PLANE - 1)
@@ -983,76 +1071,65 @@
             end_recv.at[at, block], {"sp": layer * PLANE + other},
         )
 
-    @pl.loop(0, layers)
+    def pass_on(at):
+        _, hop, way = arrival(at)
+
+        @pl.when(hop > 1)
+        def _():
+            pass_tokens(way, hop)
+
+    def attend(block):
+        attend_block(
+            block, layer, spot, queries, pairs, before, sink_ref, mixers.at[layer, 0, block]
+        )
+
+    @pl.loop(0, layers + 1)
     def _(at):
-        block, hop, way = arrival(at)
-
         @pl.when(at > 0)
         def _():
-            half = half_held.at[block]
+            block, hop, way = arrival(at - 1)
+
+            @pl.when((spot > 0) | (block == 0) | ((at > 1) & (way == 1)))
+            def _():
+                @pl.when((spot > 0) | (block > 0))
+                def _():
+                    arrive(block)
+
+                attend(block)
+
+            @pl.when((spot == 0) & (at > 1) & (way == 0))
+            def _():
+                arrive(block + 1)
+                attend(block + 1)
+
+        @pl.when(at < layers)
+        def _():
+            block, hop, way = arrival(at)
+
+            @pl.when((least == 0) & (at > 0))
+            def _():
+                pass_on(at)
 
             @pl.when(hop > 1)
             def _():
-                remote(
-                    half, half, line_send.at[way, 0], line_recv.at[way, hop - 1], {"sp": 0}
-                ).wait_recv()
-                onward = jnp.where(way == 0, layer < layers - 1, layer > 0)
-
-                @pl.when(onward & (hop < layers - 1))
-                def _():
-                    remote(
-                        half, half, line_send.at[way, hop], line_recv.at[way, hop],
-                        {"sp": (layer + 1 - 2 * way) * PLANE + spot},
-                    ).start()
-
-                remote(
-                    half, half, part_send.at[way, hop - 1], part_recv.at[way, hop - 1],
-                    {"tp": 1 - core},
-                ).start()
-
-            other_half = held.at[block, 1 - core]
-            remote(
-                other_half, other_half, part_send.at[way, hop - 1], part_recv.at[way, hop - 1],
-                {"tp": 1 - core},
-            ).wait_recv()
-
-        normalise(block, held, norm_gain_ref, normed)
-        project_block(
-            block, spot, normed, weights,
-            (row_cos_ref, row_sin_ref, block_cos_ref, block_sin_ref), queries, pairs, inputs,
-        )
-        hand_on(block).start()
-        scan_block(block, spot, inputs, drive, powers, states, carries, ends)
-        for peer in range(PLANE - 1):
-            tell(block, peer).start()
-
-        kind, half = (lax.div(at, 2), lax.rem(at, 2))
-
-        @pl.when(kind < 2)
-        def _():
-            for copy in plane_halves(
-                matrices.at[kind, spot], matrices.at[kind], layer, spot, matrix_send.at[kind],
-                matrix_recv.at[kind], half,
-            ):
-                copy.start()
-
-        @pl.when((spot > 0) | (block == 0) | ((at > 0) & (way == 1)))
-        def _():
-            @pl.when((spot > 0) | (block > 0))
+                landed(at)
+
+            project_block(
+                block, spot, normed, weights,
+                (row_cos_ref, row_sin_ref, block_cos_ref, block_sin_ref), queries, pairs, inputs,
+            )
+            hand_on(block).start()
+            scan_block(block, spot, inputs, drive, powers, states, carries, ends)
+            for peer in range(PLANE - 1):
+                tell(block, peer).start()
+
+            @pl.when((least > 0) & (at < layers - 2))
             def _():
-                arrive(block)
-
-            attend_block(
-                block, layer, spot, queries, pairs, before, sink_ref, mixers.at[layer, 0, block]
-            )
-
-        @pl.when((spot == 0) & (at > 0) & (way == 0))
-        def _():
-            arrive(block + 1)
-            attend_block(
-                block + 1, layer, spot, queries, pairs, before, sink_ref,
-                mixers.at[layer, 0, block + 1],
-            )
+                pass_on(at + 2)
+
+            @pl.when((least == 0) & (at == 2))
+            def _():
+                plane_pass(matrices.at[0], layer, spot, matrix_send.at[0], matrix_recv.at[0])
 
     @pl.when(spot == 0)
     def _():
@@ -1065,7 +1142,14 @@
         )
 
     mixers_first(0)
-    plane_pass(matrices.at[0], layer, spot, matrix_send.at[0], matrix_recv.at[0])
+
+    @pl.when(least > 0)
+    def _():
+        plane_pass(matrices.at[0], layer, spot, matrix_send.at[0], matrix_recv.at[0])
+
+    plane_first(
+        matrices.at[1, spot], matrices.at[1], layer, spot, matrix_send.at[1], matrix_recv.at[1]
+    )
     for block in range(layers):
         for peer in range(PLANE - 1):
             tell(block, peer).wait()
@@ -1079,14 +1163,6 @@
         )
 
     mixers_first(1)
-    plane_pass(matrices.at[1], layer, spot, matrix_send.at[1], matrix_recv.at[1])
-    for kind in (0, 1):
-        line_pass(
-            layers, layer, spot, 1, mixers.at[:, kind], mixer_send.at[kind], mixer_recv.at[kind]
-        )
-    for kind in (0, 1):
-        plane_landed(matrices.at[kind], spot, matrix_send.at[kind], matrix_recv.at[kind])
-
     depth = mixers.shape[-1]
     tokens = layers * rows
     half_depth, width = matrices.shape[3:]
@@ -1096,25 +1172,21 @@
     def take(at):
         block, hop, way = arrival(at)
 
-        @pl.when(hop > 1)
-        def _():
-            for kind in (0, 1):
-                columns = mixers.at[block, kind]
+        for kind in (0, 1):
+            columns = mixers.at[block, kind]
+            remote(
+                columns, columns, mixer_send.at[kind, 0, 0],
+                mixer_recv.at[kind, way, hop - 1], {"sp": 0},
+            ).wait_recv()
+            onward = jnp.where(way == 0, layer < layers - 1, layer > 0)
+
+            @pl.when(onward & (hop < layers - 1))
+            def _():
                 remote(
-                    columns, columns, mixer_send.at[kind, 0, 0],
-                    mixer_recv.at[kind, way, hop - 1], {"sp": 0},
-                ).wait_recv()
-                onward = jnp.where(way == 0, layer < layers - 1, layer > 0)
-
-                @pl.when(onward & (hop < layers - 1))
-                def _():
-                    remote(
-                        columns, columns, mixer_send.at[kind, way, hop],
-                        mixer_recv.at[kind, way, hop],
-                        {"sp": (layer + 1 - 2 * way) * PLANE + spot},
-                    ).start()
-
-        return block
+                    columns, columns, mixer_send.at[kind, way, hop],
+                    mixer_recv.at[kind, way, hop],
+                    {"sp": (layer + 1 - 2 * way) * PLANE + spot},
+                ).start()
 
     def product(block, column):
         low = pl.ds(pl.multiple_of(lax.rem(block, per) * depth, depth), depth)
@@ -1127,21 +1199,28 @@
             for kind in (0, 1)
         )
 
-    @pl.loop(0, layers - 1)
-    def _(at):
-        block = take(at)
-        for column in range(PLANE):
-            value = product(block, column)
-
-            @pl.when(at == 0)
-            def _():
-                total[column] = value
-
-            @pl.when(at > 0)
-            def _():
-                total[column] += value
-
-    last = take(jnp.int32(layers - 1))
+    for at in range(1, layers - 1):
+        take(jnp.where(at <= 2 * least, at - 1 + 2 * (at % 2), at))
+        if at == 1:
+            plane_pass(matrices.at[1], layer, spot, matrix_send.at[1], matrix_recv.at[1])
+    @pl.when(least > 0)
+    def _():
+        take(jnp.int32(layers - 1))
+
+    for kind in (0, 1):
+        plane_landed(matrices.at[kind], spot, matrix_send.at[kind], matrix_recv.at[kind])
+
+    @pl.loop(0, PLANE)
+    def _(column):
+        total[column] = sum(
+            product(arrival(jnp.int32(at))[0], column) for at in range(layers - 1)
+        )
+
+    @pl.when(least == 0)
+    def _():
+        take(jnp.int32(layers - 1))
+
+    last = arrival(jnp.int32(layers - 1))[0]
 
     def swap(column):
         return remote(
@@ -1193,39 +1272,41 @@
         for half in range(CORES):
             partial[column, half] = value[:, half]
         swap(column).start()
+        if column == 0:
+            for kind in (0, 1):
+                line_drain(
+                    layers, layer, mixers.at[layer, kind], mixers.at[:, kind],
+                    mixer_send.at[kind], mixer_recv.at[kind],
+                )
         if column > 0:
             send_column(column - 1)
     send_column(PLANE - 1)
-    for kind in (0, 1):
-        line_drain(
-            layers, layer, mixers.at[layer, kind], mixers.at[:, kind], mixer_send.at[kind],
-            mixer_recv.at[kind],
-        )
-    line_drain(layers, layer, tokens_ref.at[core], half_held, line_send, line_recv)
+    chunk_lines(
+        lambda chunk, slots, send, recv: line_drain(
+            layers, layer, slots.at[layer], slots, send, recv
+        )
+    )
     for hop in range(1, layers):
         for way, there in ((0, layer - hop >= 0), (1, layer + hop <= layers - 1)):
 
             @pl.when(there)
             def _():
-                block = held.at[layer, 0]
-                remote(
-                    block, block, part_send.at[way, hop - 1], part_recv.at[way, hop - 1],
-                    {"tp": 1 - core},
-                ).wait_send()
+                for chunk in range(chunks):
+                    part(way, hop, chunk, core).wait_send()
 
     for block in range(layers):
         hand_on(block).wait_send()
+    squares = jnp.zeros((half_rows, width), jnp.float32)
     for column in range(PLANE):
         each_landing(column)
+        for at in range(layers):
+            value = pieces[column, at].astype(jnp.float32)
+            squares = squares + value * value
     for column in range(PLANE):
         swap(column).wait_send()
         each_piece(column, lambda copy: copy.wait_send())
-    squares = jnp.zeros((half_rows, 1), jnp.float32)
-    for column in range(PLANE):
-        for at in range(layers):
-            value = pieces[column, at].astype(jnp.float32)
-            squares = squares + jnp.sum(value * value, axis=-1, keepdims=True)
-    scale = lax.rsqrt(squares / (layers * PLANE * width) + epsilon)
+    mean = jnp.sum(squares, axis=-1, keepdims=True) / (layers * PLANE * width)
+    scale = lax.rsqrt(mean + epsilon)
     for at in range(layers):
         for column in range(PLANE):
             low = (at * PLANE + column) * width
@@ -1291,10 +1372,10 @@
         out_specs=vmem,
         scratch_shapes=[
             pltpu.VMEM((2, 2, depth // 2, w_key.shape[1]), low),
-            pltpu.VMEM((layers, 2, depth // 2, pair_width), low),
+            pltpu.VMEM((layers, 2, depth // 2, width), low),
             pltpu.VMEM((layers, PLANE, 2, depth // 2, width), low),
-            pltpu.VMEM((layers, CORES, half_rows, model), low),
-            pltpu.VMEM((rows, model), low),
+            pltpu.VMEM((layers, CORES, CHUNKS, half_rows // CHUNKS, model), low),
+            pltpu.VMEM((layers, rows, model), low),
             pltpu.VMEM((groups, group_width, states), full),
             pltpu.VMEM((groups, group_width, states), full),
             pltpu.VMEM((groups, group_width, states), full),
@@ -1315,8 +1396,9 @@
             pltpu.VMEM((PLANE, layers * rows, out_width), full),
             pltpu.VMEM((PLANE, CORES, layers, half_rows, out_width), low),
             piece, piece, piece,
-            dma((11,)), dma((2, layers, 3)), dma((2, layers, 3)),
-            dma((2, layers)), dma((2, layers)), dma((2, layers)), dma((2, layers)),
+            dma((11,)), dma((layers + 1, 2)), dma((2, layers)), dma((2, layers)),
+            dma((CHUNKS, 2, layers)), dma((CHUNKS, 2, layers)),
+            dma((CHUNKS, 2, layers)), dma((CHUNKS, 2, layers)),
             dma((layers, 2, 3)), dma((layers, 2, 3)), dma((layers,)), dma((layers + 1,)),
             dma((PLANE - 1, layers)), dma((PLANE - 1, layers)),
             dma((2, 2, layers)), dma((2, 2, layers)), dma((2, 2, 3)), dma((2, 2, 3)),
@@ -1326,7 +1408,7 @@
             collective_id=0, has_side_effects=True, vmem_limit_bytes=60 * 2**20
         ),
     )(
-        tokens.reshape(CORES, half_rows, model), halved(w_query), halved(w_key), halved(w_value),
+        tokens.reshape(CORES, CHUNKS, half_rows // CHUNKS, model), halved(w_query), halved(w_key), halved(w_value),
         halved(w_state_in), jnp.swapaxes(in_re, 1, 2), jnp.swapaxes(in_im, 1, 2), out_re, out_im, halved(w_attn_out),
         halved(w_state_out), norm_gain.reshape(1, -1), out_gain.reshape(1, -1), decay_rate,
         rotation, skip_gain.reshape(1, -1), *tables, log_step, sink_logit,

time: 142 us -> 133 us (0.937)
  Pallas kernels: 140 us -> 131 us
    pallas_call x1, Pallas kernels: 140 us -> 131 us  [body(): pl.pallas_call(whole_kernel, out_shape=jax.ShapeDtypeStruct((half_rows, m...]
where the time goes in v4:
time: 133 us
  Pallas kernels  131 us (98%)
  local copies, waits for them, and re-layouts  1.87 us (1%)
    pallas_call x1, Pallas kernels, body(): pl.pallas_call(whole_kernel, out_shape=jax.ShapeDtypeStruct((half_rows, m...  131 us

profile of v4, /device:TPU:0, one launch (start us, length us, event | category | flops | bytes accessed | tf_op | source)
XLA Modules:
  0.0 132.7 jit_solution(15045727963663537862)
XLA Ops:
  0.0 130.9 %shard_map.208 = bf16[64,4096]{1,0:T(8,128)(2,1)} custom-call(bf16[2,2,32,4096]{3,2,1,0:T(8,128)(2,1)} %bitcast.12, bf16[2,128,1024]{2,1,0:T(8,128)(2,1)} %bitcast.13, bf16[2,128,256]{2,1,0:T(8,128)(2,1)} %bitcast.19, bf16[2,128,256]{2,1,0:T(8,128)(2,1)} %bitcast.20, bf16[2,128,1024]{2,1,0:T(8,128)(2,1)} %bitcast.14, f32[64,16,64]{2,1,0:T(8,128)} %bitcast.15, ...), custom_call_target="tpu_custom_call" | custom-call | tf_op jit(solution)/shard_map/pallas_call | solution.py:1368
  130.9 1.9 %copy.24 = bf16[64,4096]{1,0:T(8,128)(2,1)} copy(bf16[64,4096]{1,0:T(8,128)(2,1)} %shard_map.208) | data formatting | bytes 1048576

commit v5 on v4

--- a/solution.py
+++ b/solution.py
@@ -460,7 +460,10 @@
             barrier, inc=1, device_id={"sp": layer * PLANE + other}, device_id_type=MESH
         )
     pl.semaphore_signal(barrier, inc=1, device_id={"tp": 1 - core}, device_id_type=MESH)
-    pl.semaphore_wait(barrier, layers + 3)
+
+
+def greeted(layers):
+    pl.semaphore_wait(pltpu.get_barrier_semaphore(), layers + 3)
 
 
 def remote(source, target, send_sem, recv_sem, device):
@@ -844,6 +847,7 @@
     layers = held.shape[0]
     rows = pairs.shape[1]
     layer, spot, core = place()
+    greet(layers, layer, spot, core)
     query_width, pair_width = (queries.shape[-1], pairs.shape[-1])
     state_width = inputs.shape[-1]
     groups = in_re.shape[0]
@@ -891,7 +895,7 @@
     weights[layer, spot, :, :, middle] = packed[layer, :, :, middle]
     for copy in far_loads:
         copy.wait()
-    greet(layers, layer, spot, core)
+    greeted(layers)
 
     below, above = (layer, layers - 1 - layer)
     least = jnp.minimum(below, above)
@@ -1078,78 +1082,103 @@
         def _():
             pass_tokens(way, hop)
 
+    def send_mixer(kind, block):
+        columns = mixers.at[layer, kind, block]
+        for way, there in ((0, layer < layers - 1), (1, layer > 0)):
+
+            @pl.when(there)
+            def _():
+                remote(
+                    columns, columns, mixer_send.at[kind, block, way, 0],
+                    mixer_recv.at[kind, block, way, 0],
+                    {"sp": (layer + 1 - 2 * way) * PLANE + spot},
+                ).start()
+
     def attend(block):
         attend_block(
             block, layer, spot, queries, pairs, before, sink_ref, mixers.at[layer, 0, block]
         )
-
-    @pl.loop(0, layers + 1)
+        send_mixer(0, block)
+
+    def attend_step(at):
+        block, hop, way = arrival(at)
+
+        @pl.when((spot > 0) | (block == 0) | ((at > 0) & (way == 1)))
+        def _():
+            @pl.when((spot > 0) | (block > 0))
+            def _():
+                arrive(block)
+
+            attend(block)
+
+        @pl.when((spot == 0) & (at > 0) & (way == 0))
+        def _():
+            arrive(block + 1)
+            attend(block + 1)
+
+    def second_matrix(half):
+        for copy in plane_halves(
+            matrices.at[1, spot], matrices.at[1], layer, spot, matrix_send.at[1],
+            matrix_recv.at[1], half,
+        ):
+            copy.start()
+
+    def attend_all_but_last():
+        @pl.loop(0, layers - 1)
+        def _(at):
+            attend_step(at)
+
+    @pl.loop(0, layers)
     def _(at):
-        @pl.when(at > 0)
+        block, hop, way = arrival(at)
+        is_last = at == layers - 1
+
+        @pl.when((least == 0) & is_last)
         def _():
-            block, hop, way = arrival(at - 1)
-
-            @pl.when((spot > 0) | (block == 0) | ((at > 1) & (way == 1)))
-            def _():
-                @pl.when((spot > 0) | (block > 0))
-                def _():
-                    arrive(block)
-
-                attend(block)
-
-            @pl.when((spot == 0) & (at > 1) & (way == 0))
-            def _():
-                arrive(block + 1)
-                attend(block + 1)
-
-        @pl.when(at < layers)
+            attend_all_but_last()
+
+        @pl.when((least == 0) & (at > 0))
         def _():
-            block, hop, way = arrival(at)
-
-            @pl.when((least == 0) & (at > 0))
-            def _():
-                pass_on(at)
-
-            @pl.when(hop > 1)
-            def _():
-                landed(at)
-
-            project_block(
-                block, spot, normed, weights,
-                (row_cos_ref, row_sin_ref, block_cos_ref, block_sin_ref), queries, pairs, inputs,
-            )
-            hand_on(block).start()
-            scan_block(block, spot, inputs, drive, powers, states, carries, ends)
-            for peer in range(PLANE - 1):
-                tell(block, peer).start()
-
-            @pl.when((least > 0) & (at < layers - 2))
-            def _():
-                pass_on(at + 2)
-
-            @pl.when((least == 0) & (at == 2))
-            def _():
-                plane_pass(matrices.at[0], layer, spot, matrix_send.at[0], matrix_recv.at[0])
+            pass_on(at)
+
+        @pl.when(hop > 1)
+        def _():
+            landed(at)
+
+        project_block(
+            block, spot, normed, weights,
+            (row_cos_ref, row_sin_ref, block_cos_ref, block_sin_ref), queries, pairs, inputs,
+        )
+        hand_on(block).start()
+        scan_block(block, spot, inputs, drive, powers, states, carries, ends)
+        for peer in range(PLANE - 1):
+            tell(block, peer).start()
+
+        @pl.when((least > 0) & (at < layers - 1))
+        def _():
+            pass_on(at + 1)
+
+        @pl.when((least == 0) & (at == 2))
+        def _():
+            plane_pass(matrices.at[0], layer, spot, matrix_send.at[0], matrix_recv.at[0])
+            second_matrix(0)
+
+        @pl.when((least > 0) & is_last)
+        def _():
+            attend_all_but_last()
+
+    attend_step(jnp.int32(layers - 1))
 
     @pl.when(spot == 0)
     def _():
         arrive(layers)
 
-    def mixers_first(kind):
-        line_first(
-            layers, layer, spot, mixers.at[layer, kind], mixers.at[:, kind],
-            mixer_send.at[kind], mixer_recv.at[kind],
-        )
-
-    mixers_first(0)
-
     @pl.when(least > 0)
     def _():
         plane_pass(matrices.at[0], layer, spot, matrix_send.at[0], matrix_recv.at[0])
-
-    plane_first(
-        matrices.at[1, spot], matrices.at[1], layer, spot, matrix_send.at[1], matrix_recv.at[1]
-    )
+        second_matrix(0)
+
+    second_matrix(1)
     for block in range(layers):
         for peer in range(PLANE - 1):
             tell(block, peer).wait()
@@ -1161,8 +1190,8 @@
             block, layer, spot, inputs, states, carries, priors, powers, read, skip_ref,
             mixers.at[layer, 1, block],
         )
-
-    mixers_first(1)
+        send_mixer(1, block)
+
     depth = mixers.shape[-1]
     tokens = layers * rows
     half_depth, width = matrices.shape[3:]
@@ -1172,21 +1201,23 @@
     def take(at):
         block, hop, way = arrival(at)
 
+        onward = jnp.where(way == 0, layer < layers - 1, layer > 0)
         for kind in (0, 1):
-            columns = mixers.at[block, kind]
-            remote(
-                columns, columns, mixer_send.at[kind, 0, 0],
-                mixer_recv.at[kind, way, hop - 1], {"sp": 0},
-            ).wait_recv()
-            onward = jnp.where(way == 0, layer < layers - 1, layer > 0)
-
-            @pl.when(onward & (hop < layers - 1))
-            def _():
+            for part in range(layers):
+                at = jnp.where(2 * block < layers, part, layers - 1 - part) if kind == 0 else part
+                columns = mixers.at[block, kind, at]
                 remote(
-                    columns, columns, mixer_send.at[kind, way, hop],
-                    mixer_recv.at[kind, way, hop],
-                    {"sp": (layer + 1 - 2 * way) * PLANE + spot},
-                ).start()
+                    columns, columns, mixer_send.at[kind, at, 0, 0],
+                    mixer_recv.at[kind, at, way, hop - 1], {"sp": 0},
+                ).wait_recv()
+
+                @pl.when(onward & (hop < layers - 1))
+                def _():
+                    remote(
+                        columns, columns, mixer_send.at[kind, at, way, hop],
+                        mixer_recv.at[kind, at, way, hop],
+                        {"sp": (layer + 1 - 2 * way) * PLANE + spot},
+                    ).start()
 
     def product(block, column):
         low = pl.ds(pl.multiple_of(lax.rem(block, per) * depth, depth), depth)
@@ -1274,10 +1305,11 @@
         swap(column).start()
         if column == 0:
             for kind in (0, 1):
-                line_drain(
-                    layers, layer, mixers.at[layer, kind], mixers.at[:, kind],
-                    mixer_send.at[kind], mixer_recv.at[kind],
-                )
+                for at in range(layers):
+                    line_drain(
+                        layers, layer, mixers.at[layer, kind, at], mixers.at[:, kind, at],
+                        mixer_send.at[kind, at], mixer_recv.at[kind, at],
+                    )
         if column > 0:
             send_column(column - 1)
     send_column(PLANE - 1)
@@ -1401,7 +1433,8 @@
             dma((CHUNKS, 2, layers)), dma((CHUNKS, 2, layers)),
             dma((layers, 2, 3)), dma((layers, 2, 3)), dma((layers,)), dma((layers + 1,)),
             dma((PLANE - 1, layers)), dma((PLANE - 1, layers)),
-            dma((2, 2, layers)), dma((2, 2, layers)), dma((2, 2, 3)), dma((2, 2, 3)),
+            dma((2, layers, 2, layers)), dma((2, layers, 2, layers)),
+            dma((2, 2, 3)), dma((2, 2, 3)),
             dma((PLANE,)), dma((PLANE,)), dma((PLANE, 2, layers)), dma((PLANE, 2, layers)),
         ],
         compiler_params=pltpu.CompilerParams(

time: 133 us -> 124 us (0.932)
  Pallas kernels: 131 us -> 122 us
    pallas_call x1, Pallas kernels: 131 us -> 122 us  [body(): pl.pallas_call(whole_kernel, out_shape=jax.ShapeDtypeStruct((half_rows, m...]
where the time goes in v5:
time: 124 us
  Pallas kernels  122 us (98%)
  local copies, waits for them, and re-layouts  1.87 us (2%)
    pallas_call x1, Pallas kernels, body(): pl.pallas_call(whole_kernel, out_shape=jax.ShapeDtypeStruct((half_rows, m...  122 us

profile of v5, /device:TPU:0, one launch (start us, length us, event | category | flops | bytes accessed | tf_op | source)
XLA Modules:
  0.0 124.1 jit_solution(5177497851933064204)
XLA Ops:
  0.0 122.2 %shard_map.208 = bf16[64,4096]{1,0:T(8,128)(2,1)} custom-call(bf16[2,2,32,4096]{3,2,1,0:T(8,128)(2,1)} %bitcast.12, bf16[2,128,1024]{2,1,0:T(8,128)(2,1)} %bitcast.13, bf16[2,128,256]{2,1,0:T(8,128)(2,1)} %bitcast.19, bf16[2,128,256]{2,1,0:T(8,128)(2,1)} %bitcast.20, bf16[2,128,1024]{2,1,0:T(8,128)(2,1)} %bitcast.14, f32[64,16,64]{2,1,0:T(8,128)} %bitcast.15, ...), custom_call_target="tpu_custom_call" | custom-call | tf_op jit(solution)/shard_map/pallas_call | solution.py:1400
  122.2 1.9 %copy.24 = bf16[64,4096]{1,0:T(8,128)(2,1)} copy(bf16[64,4096]{1,0:T(8,128)(2,1)} %shard_map.208) | data formatting | bytes 1048576

commit v6 on v5

--- a/solution.py
+++ b/solution.py
@@ -1005,7 +1005,7 @@
             def _():
                 send_tokens(short)
 
-        if at == layers - 1:
+        if at == 1:
 
             @pl.when(least > 0)
             def _():

time: 124 us -> 120 us (0.968)
  Pallas kernels: 122 us -> 118 us
    pallas_call x1, Pallas kernels: 122 us -> 118 us  [body(): pl.pallas_call(whole_kernel, out_shape=jax.ShapeDtypeStruct((half_rows, m...]
where the time goes in v6:
time: 120 us
  Pallas kernels  118 us (98%)
  local copies, waits for them, and re-layouts  1.87 us (2%)
    pallas_call x1, Pallas kernels, body(): pl.pallas_call(whole_kernel, out_shape=jax.ShapeDtypeStruct((half_rows, m...  118 us

profile of v6, /device:TPU:0, one launch (start us, length us, event | category | flops | bytes accessed | tf_op | source)
XLA Modules:
  0.0 120.3 jit_solution(16066846476417194339)
XLA Ops:
  0.0 118.4 %shard_map.208 = bf16[64,4096]{1,0:T(8,128)(2,1)} custom-call(bf16[2,2,32,4096]{3,2,1,0:T(8,128)(2,1)} %bitcast.12, bf16[2,128,1024]{2,1,0:T(8,128)(2,1)} %bitcast.13, bf16[2,128,256]{2,1,0:T(8,128)(2,1)} %bitcast.19, bf16[2,128,256]{2,1,0:T(8,128)(2,1)} %bitcast.20, bf16[2,128,1024]{2,1,0:T(8,128)(2,1)} %bitcast.14, f32[64,16,64]{2,1,0:T(8,128)} %bitcast.15, ...), custom_call_target="tpu_custom_call" | custom-call | tf_op jit(solution)/shard_map/pallas_call | solution.py:1400
  118.4 1.9 %copy.24 = bf16[64,4096]{1,0:T(8,128)(2,1)} copy(bf16[64,4096]{1,0:T(8,128)(2,1)} %shard_map.208) | data formatting | bytes 1048576
